TPU v7x, 1024 devices: a whole 4x8x16 slice. The times are simulated.
1024 devices in a mesh: ra: 128 (over z, y), cb: 8 (over x, core).
Axes of the slice: x: 4, y: 8, z: 16, core: 2. Of those that a mesh axis runs over, the one named last changes fastest.
Arguments:
- tokens: bfloat16 [512, 4096], P(None, 'cb'), may hold values from -82 to 82
- gate_weight: float32 [2, 4096, 11264], P(None, 'cb', 'ra'), may hold values from -0.09375 to 0.09375
- up_weight: float32 [2, 4096, 11264], P(None, 'cb', 'ra'), may hold values from -0.09375 to 0.09375
- down_weight: float32 [2, 11264, 4096], P(None, 'ra', 'cb'), may hold values from -0.0546875 to 0.0546875
- gate_scale: float32 [2, 11264], P(None, 'ra'), may hold values from 0.5 to 2
- up_scale: float32 [2, 11264], P(None, 'ra'), may hold values from 0.5 to 2
- down_scale: float32 [2, 4096], P(None, 'cb'), may hold values from 0.5 to 2
- norm_gain: float32 [2, 4096], P(None, 'cb'), may hold values from 0.1 to 1.9
- conv_taps: float32 [2, 3, 11264], P(None, None, 'ra'), may hold values from -3 to 3
- conv_bias: float32 [2, 11264], P(None, 'ra'), may hold values from -3 to 3
Outputs:
- layer_out: bfloat16 [512, 4096], P(None, 'cb')
All inputs are finite; a program needn't handle non-finite values.
Results may differ from a plain program's by a relative error of at most 0.012.
Values may be sent and summed in bfloat16 or wider, within the bound.
No kernel may reach another device: no remote copies, remote signals or barrier semaphores. Data moves between devices by JAX's collectives and lax.ppermute only.
A program may use at most 32 MiB of HBM per device.

v0:
```python
import jax
import jax.numpy as jnp
from jax import lax
from jax.sharding import Mesh
from jax.sharding import PartitionSpec as P

D = 4096
LAYERS = 2
RA = ("ra_0", "ra_1")


norm_eps = 1e-06
residual_scale = 0.25


def sent_to_all(value, axis):
    devices = lax.axis_size(axis)
    return lax.all_to_all(
        jnp.broadcast_to(value[None], (devices, *value.shape)), axis, 0, 0, tiled=True
    )


def taken_together(value, axis):
    return sent_to_all(value, axis).sum(axis=0)


def together(arrays, axis):
    line, at, finished = (jnp.concatenate([a.reshape(-1) for a in arrays]), 0, [])
    subtotal = taken_together(line, axis)
    for a in arrays:
        finished.append(subtotal[at : at + a.size].reshape(a.shape))
        at += a.size
    return tuple(finished)


def summed_rows(value, axes, dim):
    for axis in axes:
        value = lax.psum_scatter(value, axis, scatter_dimension=dim, tiled=True)
    return value


def in_order(pieces, dim):
    lengths = list(pieces.shape[1:])
    lengths[dim] *= pieces.shape[0]
    return jnp.moveaxis(pieces, 0, dim).reshape(lengths)


def all_blocks(value, axes, sequence):
    pieces = value[None]
    for k in sequence:
        pieces = lax.all_gather(pieces, axes[k], axis=0, tiled=True)
    carried = [lax.axis_size(axes[k]) for k in reversed(sequence)]
    pieces = pieces.reshape(*carried, *value.shape)
    turned = sorted(range(len(sequence)), key=lambda place: sequence[len(sequence) - 1 - place])
    return pieces.transpose(*turned, *range(len(sequence), pieces.ndim)).reshape(-1, *value.shape)


def gathered_by_axis(value, axes, sequence, dim):
    return in_order(all_blocks(value, axes, sequence), dim)


def activate(gate, upward, taps, bias):
    padded = jnp.pad(gate, ((1, 1), (0, 0)))
    mixed = taps[0] * padded[:-2] + taps[1] * padded[1:-1] + taps[2] * padded[2:] + bias
    return (jax.nn.silu(mixed) * upward).astype(jnp.bfloat16)


def per_device(
    tokens,
    gate_weight,
    up_weight,
    down_weight,
    gate_scale,
    up_scale,
    down_scale,
    norm_gain,
    conv_taps,
    conv_bias,
):
    hstate = tokens
    for layer in range(LAYERS):
        wide = hstate.astype(jnp.float32)
        squares_part = jnp.sum(wide * wide, axis=1)
        operand = (wide * norm_gain[layer]).astype(jnp.bfloat16)
        gate_part = jnp.dot(
            operand, gate_weight[layer].astype(jnp.bfloat16), preferred_element_type=jnp.float32
        )
        up_part = jnp.dot(
            operand, up_weight[layer].astype(jnp.bfloat16), preferred_element_type=jnp.float32
        )
        gate_sum, up_sum, square_sum = together((gate_part, up_part, squares_part), "cb")
        rscale = lax.rsqrt(square_sum / D + norm_eps)[:, None]
        gate = gate_sum * rscale * gate_scale[layer]
        upward = up_sum * rscale * up_scale[layer]
        hidden = activate(gate, upward, conv_taps[layer], conv_bias[layer])
        term = jnp.dot(
            hidden, down_weight[layer].astype(jnp.bfloat16), preferred_element_type=jnp.float32
        )
        share = summed_rows(term, RA, 1)
        share_width = share.shape[1]
        offset = lax.axis_index(RA) * share_width
        wide_share = lax.dynamic_slice_in_dim(wide, offset, share_width, axis=1)
        scale_share = lax.dynamic_slice_in_dim(down_scale[layer], offset, share_width, axis=0)
        fresh = (residual_scale * wide_share + share * scale_share).astype(jnp.bfloat16)
        hstate = gathered_by_axis(fresh, RA, (0, 1), 1)
    return hstate


def solution(mesh):
    split = Mesh(mesh.devices.reshape(16, 8, mesh.shape["cb"]), ("ra_0", "ra_1", "cb"))
    return jax.shard_map(
        per_device,
        mesh=split,
        in_specs=(
            P(None, "cb"),
            P(None, "cb", RA),
            P(None, "cb", RA),
            P(None, RA, "cb"),
            P(None, RA),
            P(None, RA),
            P(None, "cb"),
            P(None, "cb"),
            P(None, None, RA),
            P(None, RA),
        ),
        out_specs=P(None, "cb"),
        check_vma=False,
    )
```

profile of v0, /device:TPU:6, one launch (start us, length us, event | category | flops | bytes accessed | tf_op | source)
XLA Modules:
  0.0 561.0 jit_solution(8129818589779628090)
XLA Ops:
  6.5 1.3 copy.38
  8.6 1.0 convert.18
  12.4 3.1 broadcast_in_dim.8
  15.4 16.8 %all-to-all-start = ((f32[8,1,90624]{2,1,0:T(1,128)}), f32[8,1,90624]{2,1,0:T(1,128)S(1)}, u32[]{:S(2)}, u32[]{:S(2)}) async-start(f32[8,1,90624]{2,1,0:T(1,128)} %broadcast_in_dim.8), calls=%async_computation | async-start | bytes 5799936 | tf_op jit(solution)/shard_map/all_to_all | solution.py:18
  32.3 1.7 convert.20
  34.0 31.9 %all-to-all-done = f32[8,1,90624]{2,1,0:T(1,128)S(1)} async-done(((f32[8,1,90624]{2,1,0:T(1,128)}), f32[8,1,90624]{2,1,0:T(1,128)S(1)}, u32[]{:S(2)}, u32[]{:S(2)}) %all-to-all-start) | async-done | bytes 2900000 | tf_op jit(solution)/shard_map/all_to_all | solution.py:18
  65.9 3.3 reduce_sum.37
  69.2 1.0 fusion.37
  71.6 2.3 fusion.4
  74.3 1.3 dynamic-slice.2
  76.2 68.9 %reduce-scatter.3.cloned.1.call-done = f32[512,32]{0,1:T(8,128)} async-done(((f32[512,512]{0,1:T(8,128)}), f32[512,32]{0,1:T(8,128)}) %reduce-scatter.3.cloned.1.call-update) | async-done | bytes 65552 | tf_op jit(solution)/shard_map/reduce_scatter | solution.py:38
  145.3 87.2 %all-reduce.7.cloned.1.call-done = f32[512,32]{0,1:T(8,128)} async-done(((f32[512,32]{0,1:T(8,128)}), f32[512,32]{0,1:T(8,128)}) %all-reduce.7.cloned.1.call-update) | async-done | bytes 65552
  233.3 31.6 %all-gather = bf16[8192,4]{0,1:T(4,128)(2,1)S(1)} all-gather(bf16[512,4]{0,1:T(4,128)(2,1)S(1)} %fusion.25), channel_id=2, replica_groups=mesh['ra_0'=16,'ra_1'=8,'cb'=8] {'ra_0'}, dimensions={0}, use_global_device_ids=true | all-gather | bytes 69632 | tf_op jit(solution)/shard_map/all_gather | solution.py:51
  265.0 25.4 %all_gather.13 = bf16[128,512,4]{1,0,2:T(8,128)(2,1)S(1)} all-gather(bf16[16,512,4]{1,0,2:T(8,128)(2,1)S(1)} %bitcast.93), channel_id=1, replica_groups=mesh['ra_0'=16,'ra_1'=8,'cb'=8] {'ra_1'}, dimensions={0}, use_global_device_ids=true | all-gather | bytes 589824 | tf_op jit(solution)/shard_map/all_gather | solution.py:51
  291.3 1.0 copy-done
  293.9 1.5 broadcast_in_dim.10
  295.4 38.3 %all_to_all.12 = f32[8,1,90624]{2,1,0:T(1,128)S(1)} all-to-all(f32[8,1,90624]{2,1,0:T(1,128)S(1)} %broadcast_in_dim.10), channel_id=1, replica_groups=mesh['ra_0'=16,'ra_1'=8,'cb'=8] {'cb'}, dimensions={0} | all-to-all | bytes 5799936 | tf_op jit(solution)/shard_map/all_to_all | solution.py:18
  333.7 2.1 reduce_sum.39
  336.5 1.5 fusion.5
  338.1 69.8 %reduce-scatter.5.cloned.1.call-done = f32[512,32]{0,1:T(8,128)} async-done(((f32[512,512]{0,1:T(8,128)}), f32[512,32]{0,1:T(8,128)}) %reduce-scatter.5.cloned.1.call-update) | async-done | bytes 65552 | tf_op jit(solution)/shard_map/reduce_scatter | solution.py:38
  408.3 86.7 %all-reduce.9.cloned.1.call-done = f32[512,32]{0,1:T(8,128)} async-done(((f32[512,32]{0,1:T(8,128)}), f32[512,32]{0,1:T(8,128)}) %all-reduce.9.cloned.1.call-update) | async-done | bytes 65552
  495.9 31.6 %all-gather.1 = bf16[8192,4]{0,1:T(4,128)(2,1)S(1)} all-gather(bf16[512,4]{0,1:T(4,128)(2,1)S(1)} %fusion.23), channel_id=3, replica_groups=mesh['ra_0'=16,'ra_1'=8,'cb'=8] {'ra_0'}, dimensions={0}, use_global_device_ids=true | all-gather | bytes 69632 | tf_op jit(solution)/shard_map/all_gather | solution.py:51
  527.5 25.4 %all_gather.15 = bf16[128,512,4]{1,0,2:T(8,128)(2,1)S(1)} all-gather(bf16[16,512,4]{1,0,2:T(8,128)(2,1)S(1)} %bitcast.94), channel_id=1, replica_groups=mesh['ra_0'=16,'ra_1'=8,'cb'=8] {'ra_1'}, dimensions={0}, use_global_device_ids=true | all-gather | bytes 589824 | tf_op jit(solution)/shard_map/all_gather | solution.py:51
  553.5 1.0 copy.47
  (74 shorter events, 11.0 us)
Async XLA Ops:
  6.5 4.4 copy-start.6
  9.6 0.7 copy-start.2
  11.0 0.7 copy-start.4
  15.4 18.5 %copy-start.10 = (f32[2,88]{1,0:T(2,128)S(1)}, f32[2,88]{1,0:T(2,128)}, u32[]{:S(2)}) copy-start(f32[2,88]{1,0:T(2,128)} %param.14) | copy-start | bytes 2116
  15.4 18.5 %copy-start.9 = (f32[2,3,88]{2,0,1:T(2,128)S(1)}, f32[2,3,88]{2,0,1:T(2,128)}, u32[]{:S(2)}) copy-start(f32[2,3,88]{2,0,1:T(2,128)} %param.18) | copy-start | bytes 6340
  15.4 18.5 %copy-start.11 = (f32[2,88]{1,0:T(2,128)S(1)}, f32[2,88]{1,0:T(2,128)}, u32[]{:S(2)}) copy-start(f32[2,88]{1,0:T(2,128)} %param.15) | copy-start | bytes 2116
  15.4 18.5 %copy-start.12 = (f32[2,88]{1,0:T(2,128)S(1)}, f32[2,88]{1,0:T(2,128)}, u32[]{:S(2)}) copy-start(f32[2,88]{1,0:T(2,128)} %param.19) | copy-start | bytes 2116
  15.4 50.5 %all-to-all-start = ((f32[8,1,90624]{2,1,0:T(1,128)}), f32[8,1,90624]{2,1,0:T(1,128)S(1)}, u32[]{:S(2)}, u32[]{:S(2)}) async-start(f32[8,1,90624]{2,1,0:T(1,128)} %broadcast_in_dim.8), calls=%async_computation | async-start | bytes 5799936 | tf_op jit(solution)/shard_map/all_to_all | solution.py:18
  32.3 112.9 %reduce-scatter.3.cloned.1.call-start = ((), (), s32[]{:S(2)}) async-start(), calls=%async_computation.4 | async-start | bytes 1114112 | tf_op jit(solution)/shard_map/reduce_scatter | solution.py:38
  71.2 5.0 copy-start.8
  74.0 158.6 %all-reduce.7.cloned.1.call-start = ((), (), s32[]{:S(2)}) async-start(), calls=%async_computation.6 | async-start | bytes 131072
  145.2 262.7 %reduce-scatter.5.cloned.1.call-start = ((), (), s32[]{:S(2)}) async-start(), calls=%async_computation.5 | async-start | bytes 1114112 | tf_op jit(solution)/shard_map/reduce_scatter | solution.py:38
  290.4 2.3 copy-start.3
  290.6 2.5 copy-start.5
  291.3 1.0 copy-start
  333.7 2.8 copy-start.7
  335.8 72.1 %copy-start.1 = (f32[16,8,512,4]{2,3,1,0:T(4,128)S(1)}, f32[16,8,512,4]{2,3,1,0:T(4,128)}, u32[]{:S(2)}) copy-start(f32[16,8,512,4]{2,3,1,0:T(4,128)} %copy-done) | copy-start | bytes 3145732
  338.0 157.0 %all-reduce.9.cloned.1.call-start = ((), (), s32[]{:S(2)}) async-start(), calls=%async_computation.7 | async-start | bytes 131072
Sparse Core Ops, SparseCore 0:
  74.1 71.0 reduce-scatter.2
  147.5 85.0 all-reduce.6
  338.2 69.6 reduce-scatter.4
  410.0 85.0 all-reduce.8
where the time goes:
time: 562 us; the launch traced here: 561 us
  waiting for transfers between devices  345 us (61%)
  blocking collectives  153 us (27%)
  starting transfers between devices  16.9 us (3%)
  local copies, waits for them, and re-layouts  16 us (3%)
  between operations  14.1 us (3%)
  other arithmetic  11.5 us (2%)
    unnamed x6, waiting for transfers between devices  174 us
    reduce_scatter x2, waiting for transfers between devices, summed_rows(): value = lax.psum_scatter(value, axis, scatter_dimension=dim, tiled=True)  139 us
    all_gather x4, blocking collectives, all_blocks(): pieces = lax.all_gather(pieces, axes[k], axis=0, tiled=True)  114 us
    all_to_all x1, blocking collectives, sent_to_all(): lax.all_to_all(jnp.broadcast_to(value[None], (devices, *value.shape)), ax...  38.3 us
    all_to_all x1, waiting for transfers between devices, sent_to_all(): lax.all_to_all(jnp.broadcast_to(value[None], (devices, *value.shape)), ax...  31.9 us
    all_to_all x1, starting transfers between devices, sent_to_all(): lax.all_to_all(jnp.broadcast_to(value[None], (devices, *value.shape)), ax...  16.8 us
  transfers between devices with their start and end apart: 5, of which 5 were waited for; matrix products, arithmetic and copies ran while one was open for 1% of the time, Pallas kernels for 0%

commit v1 on v0

v1 whole, which is shorter than its diff:
```python
import jax
import jax.numpy as jnp
from jax import lax
from jax.sharding import Mesh
from jax.sharding import PartitionSpec as P

RA = ("ra_0", "ra_1")
LANES = 128
TILE = 8

norm_eps = 1e-06
residual_scale = 0.25


def swapped(pieces, axes):
    return lax.all_to_all(pieces, axes, 0, 0, tiled=True)


def sent_to_all(value, axes):
    return swapped(jnp.broadcast_to(value[None], (lax.axis_size(axes), *value.shape)), axes)


def padded_to(value, size, axis):
    widths = [(0, 0)] * value.ndim
    widths[axis] = (0, size - value.shape[axis])
    return jnp.pad(value, widths)


def with_neighbours(rows, blocks):
    width = rows.shape[1]
    main = rows.reshape(blocks, -1, width)
    nothing = jnp.zeros((1, width), rows.dtype)
    before = jnp.concatenate([nothing, main[:-1, -1]], axis=0)[:, None]
    after = jnp.concatenate([main[1:, 0], nothing], axis=0)[:, None]
    rest = jnp.zeros((blocks, TILE - 2, width), rows.dtype)
    return jnp.concatenate([main, before, after, rest], axis=1)


def split_in_two(value):
    high = lax.reduce_precision(value, 8, 7)
    return high, value - high


def split_in_three(value):
    first, rest = split_in_two(value)
    second, third = split_in_two(rest)
    return jnp.concatenate([first, second, third], axis=0).astype(jnp.bfloat16)


def side_by_side(gate_weight, up_weight):
    return jnp.concatenate(
        [padded_to(gate_weight, LANES, 1), padded_to(up_weight, LANES, 1)], axis=1
    ).astype(jnp.bfloat16)


def with_squares(product, squares, hidden):
    high, low = split_in_two(squares)
    column = lax.broadcasted_iota(jnp.int32, product.shape, product.ndim - 1)
    product = jnp.where(column == hidden, high, product)
    return jnp.where(column == hidden + 1, low, product)


def activated(total, features, hidden, params):
    rows = total.shape[0] - TILE
    square_sum = total[:, hidden : hidden + 1] + total[:, hidden + 1 : hidden + 2]
    rscale = lax.rsqrt(square_sum / features + norm_eps)
    gate = total[:, :LANES] * rscale * params[4]
    upward = total[:rows, LANES:] * rscale[:rows] * params[5]
    main = gate[:rows]
    before = jnp.concatenate([gate[rows : rows + 1], main[:-1]], axis=0)
    after = jnp.concatenate([main[1:], gate[rows + 1 : rows + 2]], axis=0)
    mixed = params[0] * before + params[1] * main + params[2] * after + params[3]
    return (jax.nn.silu(mixed) * upward).astype(jnp.bfloat16)


def own_params(conv_taps, conv_bias, gate_scale, up_scale):
    stacked = jnp.concatenate([conv_taps, conv_bias[None], gate_scale[None], up_scale[None]], axis=0)
    return padded_to(stacked, LANES, 1)


def per_device(
    tokens,
    gate_weight,
    up_weight,
    down_weight,
    gate_scale,
    up_scale,
    down_scale,
    norm_gain,
    conv_taps,
    conv_bias,
):
    blocks_c, blocks_y, blocks_z = (lax.axis_size(a) for a in ("cb", "ra_1", "ra_0"))
    at_y, at_z = lax.axis_index("ra_1"), lax.axis_index("ra_0")
    length, width = tokens.shape
    hidden = gate_weight.shape[2]
    features = width * blocks_c
    block = length // blocks_y
    f32, bf16 = jnp.float32, jnp.bfloat16

    params_1 = own_params(conv_taps[1], conv_bias[1], gate_scale[1], up_scale[1])
    carried = split_in_three(padded_to(params_1, TILE, 0))
    carried = padded_to(carried, 2 * LANES, 1)
    packed = jnp.concatenate([side_by_side(gate_weight[1], up_weight[1]), carried], axis=0)
    packed = lax.all_gather(packed, "ra_1", axis=0)
    down_1 = lax.all_gather(padded_to(down_weight[1], LANES, 0).astype(bf16), "ra_1", axis=0)

    params_0 = own_params(conv_taps[0], conv_bias[0], gate_scale[0], up_scale[0])
    wide = tokens.astype(f32)
    squares = jnp.sum(wide * wide, axis=1, keepdims=True)
    operand = (wide * norm_gain[0]).astype(bf16)
    product = jnp.dot(
        operand, side_by_side(gate_weight[0], up_weight[0]), preferred_element_type=f32
    )
    product = with_squares(product, squares, hidden).astype(bf16)
    total = swapped(with_neighbours(product, blocks_c), "cb").astype(f32).sum(axis=0)
    inner = activated(total, features, hidden, params_0)
    inner = sent_to_all(inner, "cb").reshape(length, LANES)
    down_0 = padded_to(down_weight[0], LANES, 0).astype(bf16)
    term = jnp.dot(inner, down_0, preferred_element_type=f32).astype(bf16)
    part = swapped(with_neighbours(term, blocks_y), "ra_1").astype(f32).sum(axis=0)
    share_rows = TILE
    part = padded_to(part.astype(bf16), share_rows * blocks_z, 0)
    part = swapped(part.reshape(blocks_z, share_rows, width), "ra_0").astype(f32).sum(axis=0)

    start = block * at_y
    mains = block // share_rows
    own = lax.dynamic_slice_in_dim(tokens, start + share_rows * jnp.minimum(at_z, mains - 1), share_rows, 0)
    before = lax.dynamic_slice_in_dim(tokens, jnp.maximum(start - 1, 0), 1, 0)
    after = lax.dynamic_slice_in_dim(tokens, jnp.minimum(start + block, length - 1), 1, 0)
    row = lax.broadcasted_iota(jnp.int32, (share_rows, 1), 0)
    edge = jnp.where((row == 0) & (at_y > 0), before, jnp.zeros_like(before))
    edge = jnp.where((row == 1) & (at_y < blocks_y - 1), after, edge)
    own = jnp.where(at_z < mains, own, jnp.where(at_z == mains, edge, jnp.zeros_like(edge)))
    fresh = (residual_scale * own.astype(f32) + part * down_scale[0]).astype(bf16)
    hstate = sent_to_all(fresh, "ra_0").reshape(blocks_z * share_rows, width)[: block + TILE]

    wide = hstate.astype(f32)
    squares = jnp.sum(wide * wide, axis=1, keepdims=True)
    operand = (wide * norm_gain[1]).astype(bf16)
    product = jnp.einsum("td,ydk->ytk", operand, packed[:, :width], preferred_element_type=f32)
    product = with_squares(product, squares[None], hidden).astype(bf16)
    total = swapped(product, "cb").astype(f32).sum(axis=0)
    theirs = lax.dynamic_index_in_dim(packed, lax.axis_index("cb"), 0, keepdims=False)
    theirs = theirs[width:, :LANES].astype(f32).reshape(3, TILE, LANES)
    theirs = theirs[0] + theirs[1] + theirs[2]
    inner = activated(total, features, hidden, theirs)
    inner = sent_to_all(inner, "cb")
    term = jnp.einsum("ytk,ykf->tf", inner, down_1, preferred_element_type=f32).astype(bf16)
    share_rows = block // blocks_z
    part = swapped(term.reshape(blocks_z, share_rows, width), "ra_0").astype(f32).sum(axis=0)
    own = lax.dynamic_slice_in_dim(hstate, share_rows * at_z, share_rows, 0).astype(f32)
    fresh = (residual_scale * own + part * down_scale[1]).astype(bf16)
    fresh = sent_to_all(fresh, "ra_0").reshape(block, width)
    return sent_to_all(fresh, "ra_1").reshape(length, width)


def solution(mesh):
    split = Mesh(mesh.devices.reshape(16, 8, mesh.shape["cb"]), ("ra_0", "ra_1", "cb"))
    return jax.shard_map(
        per_device,
        mesh=split,
        in_specs=(
            P(None, "cb"),
            P(None, "cb", RA),
            P(None, "cb", RA),
            P(None, RA, "cb"),
            P(None, RA),
            P(None, RA),
            P(None, "cb"),
            P(None, "cb"),
            P(None, None, RA),
            P(None, RA),
        ),
        out_specs=P(None, "cb"),
        check_vma=False,
    )
```

time: 562 us -> 218 us (0.39)
  waiting for transfers between devices: 345 us -> 63.6 us
  blocking collectives: 153 us -> 61.3 us
  starting transfers between devices: 16.9 us -> 61 us
  other arithmetic: 11.5 us -> 3.17 us
  local copies, waits for them, and re-layouts: 16 us -> 8.93 us
    unnamed x6 -> x2, waiting for transfers between devices: 174 us -> 0.05 us
    reduce_scatter x2 -> x0, waiting for transfers between devices: 139 us -> none  [summed_rows(): value = lax.psum_scatter(value, axis, scatter_dimension=dim, tiled=True)]
    all_gather x4 -> x0, blocking collectives: 114 us -> none  [all_blocks(): pieces = lax.all_gather(pieces, axes[k], axis=0, tiled=True)]
    all_to_all x1 -> x7, starting transfers between devices: 16.8 us -> 60.9 us  [swapped(): return lax.all_to_all(pieces, axes, 0, 0, tiled=True)]
    all_to_all x1 -> x3, blocking collectives: 38.3 us -> 61.3 us  [swapped(): return lax.all_to_all(pieces, axes, 0, 0, tiled=True)]
    all_to_all x1 -> x7, waiting for transfers between devices: 31.9 us -> 53.4 us  [swapped(): return lax.all_to_all(pieces, axes, 0, 0, tiled=True)]
    all_gather x0 -> x2, waiting for transfers between devices: none -> 10.2 us  [the longest x1 10.2 us: per_device(): lax.all_gather(padded_to(down_weight[1], LANES, 0).astype(bf16), 'ra_1',...]
  transfers between devices with their start and end apart: 5 -> 9, of which waited for: 5 -> 7; matrix products, arithmetic and copies ran while one was open for 1% -> 5% of each run, Pallas kernels for 0% -> 0%
where the time goes in v1:
time: 218 us; the launch traced here: 217 us
  waiting for transfers between devices  63.6 us (29%)
  blocking collectives  61.3 us (28%)
  starting transfers between devices  61 us (28%)
  between operations  14 us (6%)
  local copies, waits for them, and re-layouts  8.93 us (4%)
  matrix products  4.9 us (2%)
  other arithmetic  3.17 us (1%)
    all_to_all x3, blocking collectives, swapped(): return lax.all_to_all(pieces, axes, 0, 0, tiled=True)  61.3 us
    all_to_all x7, starting transfers between devices, swapped(): return lax.all_to_all(pieces, axes, 0, 0, tiled=True)  60.9 us
    all_to_all x7, waiting for transfers between devices, swapped(): return lax.all_to_all(pieces, axes, 0, 0, tiled=True)  53.4 us
    all_gather x1, waiting for transfers between devices, per_device(): lax.all_gather(padded_to(down_weight[1], LANES, 0).astype(bf16), 'ra_1',...  10.2 us
  transfers between devices with their start and end apart: 9, of which 7 were waited for; matrix products, arithmetic and copies ran while one was open for 5% of the time, Pallas kernels for 0%

profile of v1, /device:TPU:6, one launch (start us, length us, event | category | flops | bytes accessed | tf_op | source)
XLA Modules:
  0.0 216.8 jit_solution(646873406982066539)
XLA Ops:
  6.5 1.2 copy.51
  7.8 1.2 copy.52
  9.8 0.8 maximum_maximum_fusion.1
  10.6 16.5 %all-to-all-start = ((bf16[8,72,256]{2,1,0:T(8,128)(2,1)}), bf16[8,72,256]{2,1,0:T(8,128)(2,1)S(1)}, u32[]{:S(2)}, u32[]{:S(2)}) async-start(bf16[8,72,256]{2,1,0:T(8,128)(2,1)} %maximum_maximum_fusion.1), calls=%async_computation | async-start | bytes 589824 | tf_op jit(solution)/shard_map/all_to_all | solution.py:16
  28.1 4.8 %all-to-all-done = bf16[8,72,256]{2,1,0:T(8,128)(2,1)S(1)} async-done(((bf16[8,72,256]{2,1,0:T(8,128)(2,1)}), bf16[8,72,256]{2,1,0:T(8,128)(2,1)S(1)}, u32[]{:S(2)}, u32[]{:S(2)}) %all-to-all-start) | async-done | bytes 294944 | tf_op jit(solution)/shard_map/all_to_all | solution.py:16
  34.1 5.4 %all-to-all-start.1 = ((bf16[8,64,128]{2,1,0:T(8,128)(2,1)}), bf16[8,64,128]{2,1,0:T(8,128)(2,1)S(1)}, u32[]{:S(2)}, u32[]{:S(2)}) async-start(bf16[8,64,128]{2,1,0:T(8,128)(2,1)} %broadcast_in_dim.134), calls=%async_computation.1 | async-start | bytes 262144 | tf_op jit(solution)/shard_map/all_to_all | solution.py:16
  39.5 4.0 %all-to-all-done.1 = bf16[8,64,128]{2,1,0:T(8,128)(2,1)S(1)} async-done(((bf16[8,64,128]{2,1,0:T(8,128)(2,1)}), bf16[8,64,128]{2,1,0:T(8,128)(2,1)S(1)}, u32[]{:S(2)}, u32[]{:S(2)}) %all-to-all-start.1) | async-done | bytes 131104 | tf_op jit(solution)/shard_map/all_to_all | solution.py:16
  44.1 28.2 %all_to_all.50 = bf16[8,72,512]{2,1,0:T(8,128)(2,1)S(1)} all-to-all(bf16[8,72,512]{2,1,0:T(8,128)(2,1)S(1)} %maximum_maximum_fusion), channel_id=1, replica_groups=mesh['ra_0'=16,'ra_1'=8,'cb'=8] {'ra_1'}, dimensions={0} | all-to-all | bytes 1179648 | tf_op jit(solution)/shard_map/all_to_all | solution.py:16
  73.0 11.6 %all-to-all-start.3 = ((bf16[16,8,512]{2,1,0:T(8,128)(2,1)}), bf16[16,8,512]{2,1,0:T(8,128)(2,1)S(1)}, u32[]{:S(2)}, u32[]{:S(2)}) async-start(bf16[16,8,512]{2,1,0:T(8,128)(2,1)} %pad_bitcast_fusion), calls=%async_computation.3 | async-start | bytes 262144 | tf_op jit(solution)/shard_map/all_to_all | solution.py:16
  84.7 13.9 %all-to-all-done.3 = bf16[16,8,512]{2,1,0:T(8,128)(2,1)S(1)} async-done(((bf16[16,8,512]{2,1,0:T(8,128)(2,1)}), bf16[16,8,512]{2,1,0:T(8,128)(2,1)S(1)}, u32[]{:S(2)}, u32[]{:S(2)}) %all-to-all-start.3) | async-done | bytes 131104 | tf_op jit(solution)/shard_map/all_to_all | solution.py:16
  99.4 3.5 %all-to-all-start.4 = ((bf16[16,8,512]{2,1,0:T(8,128)(2,1)}), bf16[16,8,512]{2,1,0:T(8,128)(2,1)S(1)}, u32[]{:S(2)}, u32[]{:S(2)}) async-start(bf16[16,8,512]{2,1,0:T(8,128)(2,1)} %broadcast_in_dim.138), calls=%async_computation.4 | async-start | bytes 262144 | tf_op jit(solution)/shard_map/all_to_all | solution.py:16
  103.7 13.1 %all-to-all-done.4 = bf16[16,8,512]{2,1,0:T(8,128)(2,1)S(1)} async-done(((bf16[16,8,512]{2,1,0:T(8,128)(2,1)}), bf16[16,8,512]{2,1,0:T(8,128)(2,1)S(1)}, u32[]{:S(2)}, u32[]{:S(2)}) %all-to-all-start.4) | async-done | bytes 131104 | tf_op jit(solution)/shard_map/all_to_all | solution.py:16
  117.0 2.8 %fusion.13 = bf16[8,72,256]{2,1,0:T(8,128)(2,1)} fusion(bf16[8,536,256]{2,1,0:T(8,128)(2,1)} %bitcast.100, bf16[72]{0:T(256)(128)(2,1)S(1)} %get-tuple-element.59, bf16[72]{0:T(256)(128)(2,1)S(1)} %get-tuple-element.58, pred[256]{0:T(512)(128)(4,1)S(1)} %get-tuple-element.62, pred[256]{0:T(512)(128)(4,1)S(1)} %get-tuple-element.63, f32[512]{0:T(512)S(1)} %bitcast.110, ...), kind=kOutput, calls=%fused_computation.11 | convolution fusion | flops 151400448 | bytes 2469888 | tf_op jit(solution)/shard_map/td,ydk->ytk/dot_general | solution.py:141
  119.8 5.5 %all-to-all-start.5 = ((bf16[8,72,256]{2,1,0:T(8,128)(2,1)}), bf16[8,72,256]{2,1,0:T(8,128)(2,1)S(1)}, u32[]{:S(2)}, u32[]{:S(2)}) async-start(bf16[8,72,256]{2,1,0:T(8,128)(2,1)} %fusion.13), calls=%async_computation.5 | async-start | bytes 589824 | tf_op jit(solution)/shard_map/all_to_all | solution.py:16
  125.3 1.0 dynamic-slice_bitcast_fusion
  126.4 4.8 %all-to-all-done.5 = bf16[8,72,256]{2,1,0:T(8,128)(2,1)S(1)} async-done(((bf16[8,72,256]{2,1,0:T(8,128)(2,1)}), bf16[8,72,256]{2,1,0:T(8,128)(2,1)S(1)}, u32[]{:S(2)}, u32[]{:S(2)}) %all-to-all-start.5) | async-done | bytes 294944 | tf_op jit(solution)/shard_map/all_to_all | solution.py:16
  132.3 5.4 %all-to-all-start.6 = ((bf16[8,64,128]{2,1,0:T(8,128)(2,1)}), bf16[8,64,128]{2,1,0:T(8,128)(2,1)S(1)}, u32[]{:S(2)}, u32[]{:S(2)}) async-start(bf16[8,64,128]{2,1,0:T(8,128)(2,1)} %broadcast_in_dim.141), calls=%async_computation.6 | async-start | bytes 262144 | tf_op jit(solution)/shard_map/all_to_all | solution.py:16
  137.7 10.2 %all-gather.7.cloned.1.call-done = bf16[1024,512]{1,0:T(8,128)(2,1)} async-done(((bf16[128,512]{1,0:T(8,128)(2,1)}), bf16[1024,512]{1,0:T(8,128)(2,1)}) %all-gather.7.cloned.1.call-update) | async-done | bytes 1048592 | tf_op jit(solution)/shard_map/all_gather | solution.py:106
  147.9 1.5 fusion.16
  150.1 13.0 %all-to-all-start.7 = ((bf16[16,4,512]{2,1,0:T(4,128)(2,1)}), bf16[16,4,512]{2,1,0:T(4,128)(2,1)S(1)}, u32[]{:S(2)}, u32[]{:S(2)}) async-start(bf16[16,4,512]{2,1,0:T(4,128)(2,1)} %reshape.75), calls=%async_computation.7 | async-start | bytes 131072 | tf_op jit(solution)/shard_map/all_to_all | solution.py:16
  163.1 12.8 %all-to-all-done.7 = bf16[16,4,512]{2,1,0:T(4,128)(2,1)S(1)} async-done(((bf16[16,4,512]{2,1,0:T(4,128)(2,1)}), bf16[16,4,512]{2,1,0:T(4,128)(2,1)S(1)}, u32[]{:S(2)}, u32[]{:S(2)}) %all-to-all-start.7) | async-done | bytes 65568 | tf_op jit(solution)/shard_map/all_to_all | solution.py:16
  176.0 15.5 %all_to_all.51 = bf16[16,4,512]{2,1,0:T(4,128)(2,1)S(1)} all-to-all(bf16[16,4,512]{2,1,0:T(4,128)(2,1)S(1)} %broadcast_in_dim.142), channel_id=1, replica_groups=mesh['ra_0'=16,'ra_1'=8,'cb'=8] {'ra_0'}, dimensions={0} | all-to-all | bytes 131072 | tf_op jit(solution)/shard_map/all_to_all | solution.py:16
  191.6 17.6 %all_to_all.52 = bf16[8,64,512]{2,1,0:T(8,128)(2,1)S(1)} all-to-all(bf16[8,64,512]{2,1,0:T(8,128)(2,1)S(1)} %broadcast_in_dim.144), channel_id=1, replica_groups=mesh['ra_0'=16,'ra_1'=8,'cb'=8] {'ra_1'}, dimensions={0} | all-to-all | bytes 1048576 | tf_op jit(solution)/shard_map/all_to_all | solution.py:16
  209.2 0.8 copy.80
  (97 shorter events, 7.8 us)
Async XLA Ops:
  6.5 2.4 %copy-start.2 = (f32[2,512]{1,0:T(2,128)S(1)}, f32[2,512]{1,0:T(2,128)}, u32[]{:S(2)}) copy-start(f32[2,512]{1,0:T(2,128)} %param.17) | copy-start | bytes 12292
  6.5 2.4 %copy-start = (bf16[512,512]{1,0:T(8,128)(2,1)S(1)}, bf16[512,512]{1,0:T(8,128)(2,1)}, u32[]{:S(2)}) copy-start(bf16[512,512]{1,0:T(8,128)(2,1)} %param.10) | copy-start | bytes 1572868
  9.5 17.6 %copy-start.4 = (f32[2,3,88]{2,0,1:T(2,128)S(1)}, f32[2,3,88]{2,0,1:T(2,128)}, u32[]{:S(2)}) copy-start(f32[2,3,88]{2,0,1:T(2,128)} %param.18) | copy-start | bytes 6340
  9.5 17.6 %copy-start.5 = (f32[2,88]{1,0:T(2,128)S(1)}, f32[2,88]{1,0:T(2,128)}, u32[]{:S(2)}) copy-start(f32[2,88]{1,0:T(2,128)} %param.19) | copy-start | bytes 2116
  9.5 17.6 %copy-start.6 = (f32[2,88]{1,0:T(2,128)S(1)}, f32[2,88]{1,0:T(2,128)}, u32[]{:S(2)}) copy-start(f32[2,88]{1,0:T(2,128)} %param.14) | copy-start | bytes 2116
  9.6 17.6 %copy-start.7 = (f32[2,88]{1,0:T(2,128)S(1)}, f32[2,88]{1,0:T(2,128)}, u32[]{:S(2)}) copy-start(f32[2,88]{1,0:T(2,128)} %param.15) | copy-start | bytes 2116
  9.6 18.4 %copy-start.1 = (f32[2,88,512]{2,1,0:T(8,128)S(1)}, f32[2,88,512]{2,1,0:T(8,128)}, u32[]{:S(2)}) copy-start(f32[2,88,512]{2,1,0:T(8,128)} %param.13) | copy-start | bytes 1081348
  10.6 22.2 %all-to-all-start = ((bf16[8,72,256]{2,1,0:T(8,128)(2,1)}), bf16[8,72,256]{2,1,0:T(8,128)(2,1)S(1)}, u32[]{:S(2)}, u32[]{:S(2)}) async-start(bf16[8,72,256]{2,1,0:T(8,128)(2,1)} %maximum_maximum_fusion.1), calls=%async_computation | async-start | bytes 589824 | tf_op jit(solution)/shard_map/all_to_all | solution.py:16
  27.1 89.9 %all-gather.5.cloned.1.call-start = ((), (), s32[]{:S(2)}) async-start(), calls=%async_computation.10 | async-start | bytes 2469888 | tf_op jit(solution)/shard_map/all_gather | solution.py:105
  34.1 9.4 %all-to-all-start.1 = ((bf16[8,64,128]{2,1,0:T(8,128)(2,1)}), bf16[8,64,128]{2,1,0:T(8,128)(2,1)S(1)}, u32[]{:S(2)}, u32[]{:S(2)}) async-start(bf16[8,64,128]{2,1,0:T(8,128)(2,1)} %broadcast_in_dim.134), calls=%async_computation.1 | async-start | bytes 262144 | tf_op jit(solution)/shard_map/all_to_all | solution.py:16
  44.1 40.7 %copy-start.3 = (f32[2,512]{1,0:T(2,128)S(1)}, f32[2,512]{1,0:T(2,128)}, u32[]{:S(2)}) copy-start(f32[2,512]{1,0:T(2,128)} %param.16) | copy-start | bytes 12292
  73.0 25.6 %all-to-all-start.3 = ((bf16[16,8,512]{2,1,0:T(8,128)(2,1)}), bf16[16,8,512]{2,1,0:T(8,128)(2,1)S(1)}, u32[]{:S(2)}, u32[]{:S(2)}) async-start(bf16[16,8,512]{2,1,0:T(8,128)(2,1)} %pad_bitcast_fusion), calls=%async_computation.3 | async-start | bytes 262144 | tf_op jit(solution)/shard_map/all_to_all | solution.py:16
  99.4 17.4 %all-to-all-start.4 = ((bf16[16,8,512]{2,1,0:T(8,128)(2,1)}), bf16[16,8,512]{2,1,0:T(8,128)(2,1)S(1)}, u32[]{:S(2)}, u32[]{:S(2)}) async-start(bf16[16,8,512]{2,1,0:T(8,128)(2,1)} %broadcast_in_dim.138), calls=%async_computation.4 | async-start | bytes 262144 | tf_op jit(solution)/shard_map/all_to_all | solution.py:16
  102.9 45.0 %all-gather.7.cloned.1.call-start = ((), (), s32[]{:S(2)}) async-start(), calls=%async_computation.11 | async-start | bytes 1179648 | tf_op jit(solution)/shard_map/all_gather | solution.py:106
  119.8 11.3 %all-to-all-start.5 = ((bf16[8,72,256]{2,1,0:T(8,128)(2,1)}), bf16[8,72,256]{2,1,0:T(8,128)(2,1)S(1)}, u32[]{:S(2)}, u32[]{:S(2)}) async-start(bf16[8,72,256]{2,1,0:T(8,128)(2,1)} %fusion.13), calls=%async_computation.5 | async-start | bytes 589824 | tf_op jit(solution)/shard_map/all_to_all | solution.py:16
  132.3 15.5 %all-to-all-start.6 = ((bf16[8,64,128]{2,1,0:T(8,128)(2,1)}), bf16[8,64,128]{2,1,0:T(8,128)(2,1)S(1)}, u32[]{:S(2)}, u32[]{:S(2)}) async-start(bf16[8,64,128]{2,1,0:T(8,128)(2,1)} %broadcast_in_dim.141), calls=%async_computation.6 | async-start | bytes 262144 | tf_op jit(solution)/shard_map/all_to_all | solution.py:16
  150.1 25.8 %all-to-all-start.7 = ((bf16[16,4,512]{2,1,0:T(4,128)(2,1)}), bf16[16,4,512]{2,1,0:T(4,128)(2,1)S(1)}, u32[]{:S(2)}, u32[]{:S(2)}) async-start(bf16[16,4,512]{2,1,0:T(4,128)(2,1)} %reshape.75), calls=%async_computation.7 | async-start | bytes 131072 | tf_op jit(solution)/shard_map/all_to_all | solution.py:16
Sparse Core Ops, SparseCore 0:
  30.5 55.5 all-gather.4
  106.4 41.4 all-gather.6

commit v2 on v1

--- a/solution.py
+++ b/solution.py
@@ -99,11 +99,17 @@
     f32, bf16 = jnp.float32, jnp.bfloat16
 
     params_1 = own_params(conv_taps[1], conv_bias[1], gate_scale[1], up_scale[1])
-    carried = split_in_three(padded_to(params_1, TILE, 0))
-    carried = padded_to(carried, 2 * LANES, 1)
-    packed = jnp.concatenate([side_by_side(gate_weight[1], up_weight[1]), carried], axis=0)
+    carried = padded_to(split_in_three(padded_to(params_1, TILE, 0)), width, 1)
+    packed = jnp.concatenate(
+        [
+            gate_weight[1].T.astype(bf16),
+            up_weight[1].T.astype(bf16),
+            down_weight[1].astype(bf16),
+            carried,
+        ],
+        axis=0,
+    )
     packed = lax.all_gather(packed, "ra_1", axis=0)
-    down_1 = lax.all_gather(padded_to(down_weight[1], LANES, 0).astype(bf16), "ra_1", axis=0)
 
     params_0 = own_params(conv_taps[0], conv_bias[0], gate_scale[0], up_scale[0])
     wide = tokens.astype(f32)
@@ -138,15 +144,25 @@
     wide = hstate.astype(f32)
     squares = jnp.sum(wide * wide, axis=1, keepdims=True)
     operand = (wide * norm_gain[1]).astype(bf16)
-    product = jnp.einsum("td,ydk->ytk", operand, packed[:, :width], preferred_element_type=f32)
+    product = jnp.concatenate(
+        [
+            padded_to(
+                jnp.einsum("td,ykd->ytk", operand, weight, preferred_element_type=f32), LANES, 2
+            )
+            for weight in (packed[:, :hidden], packed[:, hidden : 2 * hidden])
+        ],
+        axis=2,
+    )
     product = with_squares(product, squares[None], hidden).astype(bf16)
     total = swapped(product, "cb").astype(f32).sum(axis=0)
     theirs = lax.dynamic_index_in_dim(packed, lax.axis_index("cb"), 0, keepdims=False)
-    theirs = theirs[width:, :LANES].astype(f32).reshape(3, TILE, LANES)
+    theirs = theirs[3 * hidden :, :LANES].astype(f32).reshape(3, TILE, LANES)
     theirs = theirs[0] + theirs[1] + theirs[2]
     inner = activated(total, features, hidden, theirs)
     inner = sent_to_all(inner, "cb")
-    term = jnp.einsum("ytk,ykf->tf", inner, down_1, preferred_element_type=f32).astype(bf16)
+    down_1 = packed[:, 2 * hidden : 3 * hidden]
+    term = jnp.einsum("ytk,ykf->tf", inner[:, :, :hidden], down_1, preferred_element_type=f32)
+    term = term.astype(bf16)
     share_rows = block // blocks_z
     part = swapped(term.reshape(blocks_z, share_rows, width), "ra_0").astype(f32).sum(axis=0)
     own = lax.dynamic_slice_in_dim(hstate, share_rows * at_z, share_rows, 0).astype(f32)

time: 218 us -> 205 us (0.940)
  starting transfers between devices: 61 us -> 40.7 us
  blocking collectives: 61.3 us -> 78.9 us
  waiting for transfers between devices: 63.6 us -> 49.5 us
  other arithmetic: 3.17 us -> 7.75 us
  local copies, waits for them, and re-layouts: 8.93 us -> 6.04 us
    all_to_all x7 -> x5, starting transfers between devices: 60.9 us -> 40.7 us  [swapped(): return lax.all_to_all(pieces, axes, 0, 0, tiled=True)]
    all_to_all x3 -> x5, blocking collectives: 61.3 us -> 78.9 us  [swapped(): return lax.all_to_all(pieces, axes, 0, 0, tiled=True)]
    all_gather x1 -> x0, waiting for transfers between devices: 10.2 us -> none  [per_device(): lax.all_gather(padded_to(down_weight[1], LANES, 0).astype(bf16), 'ra_1',...]
    all_to_all x7 -> x5, waiting for transfers between devices: 53.4 us -> 49.4 us  [swapped(): return lax.all_to_all(pieces, axes, 0, 0, tiled=True)]
    unnamed x25 -> x19, local copies, waits for them, and re-layouts: 3.23 us -> 0.86 us
    dot_general x2 -> x3, matrix products: 4.31 us -> 4.43 us  [the longest x2 3.04 us: per_device(): jnp.einsum('td,ykd->ytk', operand, weight, preferred_element_type=f32)]
  transfers between devices with their start and end apart: 9 -> 6, of which waited for: 7 -> 5; matrix products, arithmetic and copies ran while one was open for 5% -> 3% of each run, Pallas kernels for 0% -> 0%
where the time goes in v2:
time: 205 us; the launch traced here: 203 us
  blocking collectives  78.9 us (38%)
  waiting for transfers between devices  49.5 us (24%)
  starting transfers between devices  40.7 us (20%)
  between operations  13.9 us (7%)
  other arithmetic  7.75 us (4%)
  matrix products  6.13 us (3%)
  local copies, waits for them, and re-layouts  6.04 us (3%)
    all_to_all x5, blocking collectives, swapped(): return lax.all_to_all(pieces, axes, 0, 0, tiled=True)  78.9 us
    all_to_all x5, waiting for transfers between devices, swapped(): return lax.all_to_all(pieces, axes, 0, 0, tiled=True)  49.4 us
    all_to_all x5, starting transfers between devices, swapped(): return lax.all_to_all(pieces, axes, 0, 0, tiled=True)  40.7 us
  transfers between devices with their start and end apart: 6, of which 5 were waited for; matrix products, arithmetic and copies ran while one was open for 3% of the time, Pallas kernels for 0%

profile of v2, /device:TPU:6, one launch (start us, length us, event | category | flops | bytes accessed | tf_op | source)
XLA Modules:
  0.0 203.0 jit_solution(662382923861713407)
XLA Ops:
  6.5 1.0 convert.33
  7.6 1.0 convert.34
  9.3 1.2 fusion.3
  10.7 1.4 fusion.1
  13.1 16.5 %all-to-all-start = ((bf16[8,72,256]{2,1,0:T(8,128)(2,1)}), bf16[8,72,256]{2,1,0:T(8,128)(2,1)S(1)}, u32[]{:S(2)}, u32[]{:S(2)}) async-start(bf16[8,72,256]{2,1,0:T(8,128)(2,1)} %maximum_maximum_fusion.1), calls=%async_computation | async-start | bytes 589824 | tf_op jit(solution)/shard_map/all_to_all | solution.py:16
  30.6 4.8 %all-to-all-done = bf16[8,72,256]{2,1,0:T(8,128)(2,1)S(1)} async-done(((bf16[8,72,256]{2,1,0:T(8,128)(2,1)}), bf16[8,72,256]{2,1,0:T(8,128)(2,1)S(1)}, u32[]{:S(2)}, u32[]{:S(2)}) %all-to-all-start) | async-done | bytes 294944 | tf_op jit(solution)/shard_map/all_to_all | solution.py:16
  35.9 8.5 %all_to_all.50 = bf16[8,64,128]{2,1,0:T(8,128)(2,1)S(1)} all-to-all(bf16[8,64,128]{2,1,0:T(8,128)(2,1)S(1)} %broadcast_in_dim.134), channel_id=1, replica_groups=mesh['ra_0'=16,'ra_1'=8,'cb'=8] {'cb'}, dimensions={0} | all-to-all | bytes 262144 | tf_op jit(solution)/shard_map/all_to_all | solution.py:16
  45.0 27.9 %all_to_all.51 = bf16[8,72,512]{2,1,0:T(8,128)(2,1)S(1)} all-to-all(bf16[8,72,512]{2,1,0:T(8,128)(2,1)S(1)} %maximum_maximum_fusion), channel_id=1, replica_groups=mesh['ra_0'=16,'ra_1'=8,'cb'=8] {'ra_1'}, dimensions={0} | all-to-all | bytes 1179648 | tf_op jit(solution)/shard_map/all_to_all | solution.py:16
  73.7 11.8 %all-to-all-start.3 = ((bf16[16,8,512]{2,1,0:T(8,128)(2,1)}), bf16[16,8,512]{2,1,0:T(8,128)(2,1)S(1)}, u32[]{:S(2)}, u32[]{:S(2)}) async-start(bf16[16,8,512]{2,1,0:T(8,128)(2,1)} %pad_bitcast_fusion), calls=%async_computation.3 | async-start | bytes 262144 | tf_op jit(solution)/shard_map/all_to_all | solution.py:16
  86.3 13.3 %all-to-all-done.3 = bf16[16,8,512]{2,1,0:T(8,128)(2,1)S(1)} async-done(((bf16[16,8,512]{2,1,0:T(8,128)(2,1)}), bf16[16,8,512]{2,1,0:T(8,128)(2,1)S(1)}, u32[]{:S(2)}, u32[]{:S(2)}) %all-to-all-start.3) | async-done | bytes 131104 | tf_op jit(solution)/shard_map/all_to_all | solution.py:16
  101.0 3.5 %all-to-all-start.4 = ((bf16[16,8,512]{2,1,0:T(8,128)(2,1)}), bf16[16,8,512]{2,1,0:T(8,128)(2,1)S(1)}, u32[]{:S(2)}, u32[]{:S(2)}) async-start(bf16[16,8,512]{2,1,0:T(8,128)(2,1)} %broadcast_in_dim.138), calls=%async_computation.4 | async-start | bytes 262144 | tf_op jit(solution)/shard_map/all_to_all | solution.py:16
  104.5 13.9 %all-to-all-done.4 = bf16[16,8,512]{2,1,0:T(8,128)(2,1)S(1)} async-done(((bf16[16,8,512]{2,1,0:T(8,128)(2,1)}), bf16[16,8,512]{2,1,0:T(8,128)(2,1)S(1)}, u32[]{:S(2)}, u32[]{:S(2)}) %all-to-all-start.4) | async-done | bytes 131104 | tf_op jit(solution)/shard_map/all_to_all | solution.py:16
  118.6 1.5 convolution_bitcast_fusion.1
  120.2 1.5 convolution_bitcast_fusion
  121.7 0.8 fusion.10
  122.5 5.5 %all-to-all-start.5 = ((bf16[8,72,256]{2,1,0:T(8,128)(2,1)}), bf16[8,72,256]{2,1,0:T(8,128)(2,1)S(1)}, u32[]{:S(2)}, u32[]{:S(2)}) async-start(bf16[8,72,256]{2,1,0:T(8,128)(2,1)} %fusion.10), calls=%async_computation.5 | async-start | bytes 589824 | tf_op jit(solution)/shard_map/all_to_all | solution.py:16
  128.0 1.0 dynamic-slice_bitcast_fusion
  129.1 4.7 %all-to-all-done.5 = bf16[8,72,256]{2,1,0:T(8,128)(2,1)S(1)} async-done(((bf16[8,72,256]{2,1,0:T(8,128)(2,1)}), bf16[8,72,256]{2,1,0:T(8,128)(2,1)S(1)}, u32[]{:S(2)}, u32[]{:S(2)}) %all-to-all-start.5) | async-done | bytes 294944 | tf_op jit(solution)/shard_map/all_to_all | solution.py:16
  134.4 8.5 %all_to_all.52 = bf16[8,64,128]{2,1,0:T(8,128)(2,1)S(1)} all-to-all(bf16[8,64,128]{2,1,0:T(8,128)(2,1)S(1)} %broadcast_in_dim.141), channel_id=1, replica_groups=mesh['ra_0'=16,'ra_1'=8,'cb'=8] {'cb'}, dimensions={0} | all-to-all | bytes 262144 | tf_op jit(solution)/shard_map/all_to_all | solution.py:16
  142.9 1.4 fusion.2
  144.9 3.5 %all-to-all-start.7 = ((bf16[16,4,512]{2,1,0:T(4,128)(2,1)}), bf16[16,4,512]{2,1,0:T(4,128)(2,1)S(1)}, u32[]{:S(2)}, u32[]{:S(2)}) async-start(bf16[16,4,512]{2,1,0:T(4,128)(2,1)} %reshape.78), calls=%async_computation.7 | async-start | bytes 131072 | tf_op jit(solution)/shard_map/all_to_all | solution.py:16
  148.5 12.7 %all-to-all-done.7 = bf16[16,4,512]{2,1,0:T(4,128)(2,1)S(1)} async-done(((bf16[16,4,512]{2,1,0:T(4,128)(2,1)}), bf16[16,4,512]{2,1,0:T(4,128)(2,1)S(1)}, u32[]{:S(2)}, u32[]{:S(2)}) %all-to-all-start.7) | async-done | bytes 65568 | tf_op jit(solution)/shard_map/all_to_all | solution.py:16
  161.3 15.5 %all_to_all.53 = bf16[16,4,512]{2,1,0:T(4,128)(2,1)S(1)} all-to-all(bf16[16,4,512]{2,1,0:T(4,128)(2,1)S(1)} %broadcast_in_dim.142), channel_id=1, replica_groups=mesh['ra_0'=16,'ra_1'=8,'cb'=8] {'ra_0'}, dimensions={0} | all-to-all | bytes 131072 | tf_op jit(solution)/shard_map/all_to_all | solution.py:16
  176.9 18.4 %all_to_all.54 = bf16[8,64,512]{2,1,0:T(8,128)(2,1)S(1)} all-to-all(bf16[8,64,512]{2,1,0:T(8,128)(2,1)S(1)} %broadcast_in_dim.144), channel_id=1, replica_groups=mesh['ra_0'=16,'ra_1'=8,'cb'=8] {'ra_1'}, dimensions={0} | all-to-all | bytes 1048576 | tf_op jit(solution)/shard_map/all_to_all | solution.py:16
  (89 shorter events, 9.0 us)
Async XLA Ops:
  10.6 19.0 %copy-start.2 = (f32[2,3,88]{2,0,1:T(2,128)S(1)}, f32[2,3,88]{2,0,1:T(2,128)}, u32[]{:S(2)}) copy-start(f32[2,3,88]{2,0,1:T(2,128)} %param.18) | copy-start | bytes 6340
  10.6 19.0 %copy-start.3 = (f32[2,88]{1,0:T(2,128)S(1)}, f32[2,88]{1,0:T(2,128)}, u32[]{:S(2)}) copy-start(f32[2,88]{1,0:T(2,128)} %param.19) | copy-start | bytes 2116
  10.6 19.1 %copy-start.4 = (f32[2,88]{1,0:T(2,128)S(1)}, f32[2,88]{1,0:T(2,128)}, u32[]{:S(2)}) copy-start(f32[2,88]{1,0:T(2,128)} %param.14) | copy-start | bytes 2116
  10.6 19.1 %copy-start.5 = (f32[2,88]{1,0:T(2,128)S(1)}, f32[2,88]{1,0:T(2,128)}, u32[]{:S(2)}) copy-start(f32[2,88]{1,0:T(2,128)} %param.15) | copy-start | bytes 2116
  10.6 19.1 %copy-start = (f32[2,88,512]{2,1,0:T(8,128)S(1)}, f32[2,88,512]{2,1,0:T(8,128)}, u32[]{:S(2)}) copy-start(f32[2,88,512]{2,1,0:T(8,128)} %param.13) | copy-start | bytes 1081348
  13.1 22.2 %all-to-all-start = ((bf16[8,72,256]{2,1,0:T(8,128)(2,1)}), bf16[8,72,256]{2,1,0:T(8,128)(2,1)S(1)}, u32[]{:S(2)}, u32[]{:S(2)}) async-start(bf16[8,72,256]{2,1,0:T(8,128)(2,1)} %maximum_maximum_fusion.1), calls=%async_computation | async-start | bytes 589824 | tf_op jit(solution)/shard_map/all_to_all | solution.py:16
  29.6 89.0 %all-gather.3.cloned.1.call-start = ((), (), s32[]{:S(2)}) async-start(), calls=%async_computation.10 | async-start | bytes 2654208 | tf_op jit(solution)/shard_map/all_gather | solution.py:112
  35.9 50.3 %copy-start.1 = (f32[2,512]{1,0:T(2,128)S(1)}, f32[2,512]{1,0:T(2,128)}, u32[]{:S(2)}) copy-start(f32[2,512]{1,0:T(2,128)} %param.16) | copy-start | bytes 12292
  73.7 25.9 %all-to-all-start.3 = ((bf16[16,8,512]{2,1,0:T(8,128)(2,1)}), bf16[16,8,512]{2,1,0:T(8,128)(2,1)S(1)}, u32[]{:S(2)}, u32[]{:S(2)}) async-start(bf16[16,8,512]{2,1,0:T(8,128)(2,1)} %pad_bitcast_fusion), calls=%async_computation.3 | async-start | bytes 262144 | tf_op jit(solution)/shard_map/all_to_all | solution.py:16
  101.0 17.4 %all-to-all-start.4 = ((bf16[16,8,512]{2,1,0:T(8,128)(2,1)}), bf16[16,8,512]{2,1,0:T(8,128)(2,1)S(1)}, u32[]{:S(2)}, u32[]{:S(2)}) async-start(bf16[16,8,512]{2,1,0:T(8,128)(2,1)} %broadcast_in_dim.138), calls=%async_computation.4 | async-start | bytes 262144 | tf_op jit(solution)/shard_map/all_to_all | solution.py:16
  122.5 11.3 %all-to-all-start.5 = ((bf16[8,72,256]{2,1,0:T(8,128)(2,1)}), bf16[8,72,256]{2,1,0:T(8,128)(2,1)S(1)}, u32[]{:S(2)}, u32[]{:S(2)}) async-start(bf16[8,72,256]{2,1,0:T(8,128)(2,1)} %fusion.10), calls=%async_computation.5 | async-start | bytes 589824 | tf_op jit(solution)/shard_map/all_to_all | solution.py:16
  144.9 16.3 %all-to-all-start.7 = ((bf16[16,4,512]{2,1,0:T(4,128)(2,1)}), bf16[16,4,512]{2,1,0:T(4,128)(2,1)S(1)}, u32[]{:S(2)}, u32[]{:S(2)}) async-start(bf16[16,4,512]{2,1,0:T(4,128)(2,1)} %reshape.78), calls=%async_computation.7 | async-start | bytes 131072 | tf_op jit(solution)/shard_map/all_to_all | solution.py:16
Sparse Core Ops, SparseCore 0:
  33.0 56.2 all-gather.2

commit v3 on v2

--- a/solution.py
+++ b/solution.py
@@ -4,6 +4,7 @@
 from jax.sharding import Mesh
 from jax.sharding import PartitionSpec as P
 
+
 RA = ("ra_0", "ra_1")
 LANES = 128
 TILE = 8
@@ -17,13 +18,28 @@
 
 
 def sent_to_all(value, axes):
-    return swapped(jnp.broadcast_to(value[None], (lax.axis_size(axes), *value.shape)), axes)
+    copies = jnp.broadcast_to(value[None], (lax.axis_size(axes), *value.shape))
+    return swapped(copies, axes)
 
 
 def padded_to(value, size, axis):
     widths = [(0, 0)] * value.ndim
     widths[axis] = (0, size - value.shape[axis])
     return jnp.pad(value, widths)
+
+
+def gathered_in_steps(own, axis):
+    size = lax.axis_size(axis)
+
+    def taken_from(value, away):
+        return lax.ppermute(value, axis, [((i + away) % size, i) for i in range(size)])
+
+    far = taken_from(own, 4)
+    ahead = taken_from(own, 2)
+    behind = taken_from(own, -2)
+    odd_ahead = taken_from(jnp.concatenate([own, ahead]), 1)
+    odd_behind = taken_from(jnp.concatenate([own, behind]), -1)
+    return jnp.concatenate([own, ahead, behind, odd_ahead, odd_behind, far])
 
 
 def with_neighbours(rows, blocks):
@@ -78,7 +94,7 @@
     return padded_to(stacked, LANES, 1)
 
 
-def per_device(
+def both_layers(
     tokens,
     gate_weight,
     up_weight,
@@ -109,7 +125,7 @@
         ],
         axis=0,
     )
-    packed = lax.all_gather(packed, "ra_1", axis=0)
+    packed = gathered_in_steps(packed[None], "ra_1")
 
     params_0 = own_params(conv_taps[0], conv_bias[0], gate_scale[0], up_scale[0])
     wide = tokens.astype(f32)
@@ -174,7 +190,7 @@
 def solution(mesh):
     split = Mesh(mesh.devices.reshape(16, 8, mesh.shape["cb"]), ("ra_0", "ra_1", "cb"))
     return jax.shard_map(
-        per_device,
+        both_layers,
         mesh=split,
         in_specs=(
             P(None, "cb"),

time: 205 us -> 215 us (1.049)
  starting transfers between devices: 40.7 us -> 72.1 us
  blocking collectives: 78.9 us -> 52 us
  between operations: 13.9 us -> 0.59 us
  waiting for transfers between devices: 49.5 us -> 61.3 us
  local copies, waits for them, and re-layouts: 6.04 us -> 11.6 us
    all_to_all x5 -> x3, blocking collectives: 78.9 us -> 52 us  [swapped(): return lax.all_to_all(pieces, axes, 0, 0, tiled=True)]
    ppermute x0 -> x5, starting transfers between devices: none -> 21.5 us  [taken_from(): lax.ppermute(value, axis, [((i + away) % size, i) for i in range(size)])]
    ppermute x0 -> x5, waiting for transfers between devices: none -> 16.2 us  [taken_from(): lax.ppermute(value, axis, [((i + away) % size, i) for i in range(size)])]
    all_to_all x5 -> x7, starting transfers between devices: 40.7 us -> 50.7 us  [swapped(): return lax.all_to_all(pieces, axes, 0, 0, tiled=True)]
    all_to_all x5 -> x7, waiting for transfers between devices: 49.4 us -> 45.1 us  [swapped(): return lax.all_to_all(pieces, axes, 0, 0, tiled=True)]
    unnamed x19 -> x23, local copies, waits for them, and re-layouts: 0.86 us -> 4.03 us
  transfers between devices with their start and end apart: 6 -> 12, of which waited for: 5 -> 8; matrix products, arithmetic and copies ran while one was open for 3% -> 5% of each run, Pallas kernels for 0% -> 0%
where the time goes in v3:
time: 215 us; the launch traced here: 213 us
  starting transfers between devices  72.1 us (34%)
  waiting for transfers between devices  61.3 us (29%)
  blocking collectives  52 us (24%)
  local copies, waits for them, and re-layouts  11.6 us (5%)
  other arithmetic  9.53 us (4%)
  matrix products  6.13 us (3%)
    all_to_all x3, blocking collectives, swapped(): return lax.all_to_all(pieces, axes, 0, 0, tiled=True)  52 us
    all_to_all x7, starting transfers between devices, swapped(): return lax.all_to_all(pieces, axes, 0, 0, tiled=True)  50.7 us
    all_to_all x7, waiting for transfers between devices, swapped(): return lax.all_to_all(pieces, axes, 0, 0, tiled=True)  45.1 us
    ppermute x5, starting transfers between devices, taken_from(): lax.ppermute(value, axis, [((i + away) % size, i) for i in range(size)])  21.5 us
    ppermute x5, waiting for transfers between devices, taken_from(): lax.ppermute(value, axis, [((i + away) % size, i) for i in range(size)])  16.2 us
  transfers between devices with their start and end apart: 12, of which 8 were waited for; matrix products, arithmetic and copies ran while one was open for 5% of the time, Pallas kernels for 0%

profile of v3, /device:TPU:6, one launch (start us, length us, event | category | flops | bytes accessed | tf_op | source)
XLA Modules:
  0.0 213.2 jit_solution(8886128423139968906)
XLA Ops:
  6.6 16.5 %all-to-all-start = ((bf16[8,72,256]{2,1,0:T(8,128)(2,1)}), bf16[8,72,256]{2,1,0:T(8,128)(2,1)S(1)}, u32[]{:S(2)}, u32[]{:S(2)}) async-start(bf16[8,72,256]{2,1,0:T(8,128)(2,1)} %maximum_maximum_fusion.1), calls=%async_computation | async-start | bytes 589824 | tf_op jit(solution)/shard_map/all_to_all | solution.py:17
  23.2 5.6 %all-to-all-done = bf16[8,72,256]{2,1,0:T(8,128)(2,1)S(1)} async-done(((bf16[8,72,256]{2,1,0:T(8,128)(2,1)}), bf16[8,72,256]{2,1,0:T(8,128)(2,1)S(1)}, u32[]{:S(2)}, u32[]{:S(2)}) %all-to-all-start) | async-done | bytes 294944 | tf_op jit(solution)/shard_map/all_to_all | solution.py:17
  30.0 5.4 %all-to-all-start.1 = ((bf16[8,64,128]{2,1,0:T(8,128)(2,1)}), bf16[8,64,128]{2,1,0:T(8,128)(2,1)S(1)}, u32[]{:S(2)}, u32[]{:S(2)}) async-start(bf16[8,64,128]{2,1,0:T(8,128)(2,1)} %broadcast_in_dim.137), calls=%async_computation.1 | async-start | bytes 262144 | tf_op jit(solution)/shard_map/all_to_all | solution.py:17
  35.4 4.0 %all-to-all-done.1 = bf16[8,64,128]{2,1,0:T(8,128)(2,1)S(1)} async-done(((bf16[8,64,128]{2,1,0:T(8,128)(2,1)}), bf16[8,64,128]{2,1,0:T(8,128)(2,1)S(1)}, u32[]{:S(2)}, u32[]{:S(2)}) %all-to-all-start.1) | async-done | bytes 131104 | tf_op jit(solution)/shard_map/all_to_all | solution.py:17
  40.9 3.5 %all-to-all-start.2 = ((bf16[8,72,512]{2,1,0:T(8,128)(2,1)}), bf16[8,72,512]{2,1,0:T(8,128)(2,1)S(1)}, u32[]{:S(2)}, u32[]{:S(2)}) async-start(bf16[8,72,512]{2,1,0:T(8,128)(2,1)} %maximum_maximum_fusion), calls=%async_computation.2 | async-start | bytes 1179648 | tf_op jit(solution)/shard_map/all_to_all | solution.py:17
  44.5 6.0 %collective-permute-start = (bf16[1,288,512]{2,1,0:T(8,128)(2,1)S(1)}, bf16[1,288,512]{2,1,0:T(8,128)(2,1)S(1)}, u32[]{:S(2)}, u32[]{:S(2)}) collective-permute-start(bf16[1,288,512]{2,1,0:T(8,128)(2,1)S(1)} %maximum_bitcast_fusion), channel_id=1, source_target_pairs={{16,0},{24,8},{32,16},{40,24},{48,32},{56,40},{0,48},{8,56},{17,1}... | collective-permute-start | bytes 884744 | tf_op jit(solution)/shard_map/ppermute | solution.py:35
  50.4 1.9 collective-permute-start.1
  52.4 6.6 %collective-permute-start.4 = (bf16[1,288,512]{2,1,0:T(8,128)(2,1)S(1)}, bf16[1,288,512]{2,1,0:T(8,128)(2,1)}, u32[]{:S(2)}, u32[]{:S(2)}) collective-permute-start(bf16[1,288,512]{2,1,0:T(8,128)(2,1)S(1)} %maximum_bitcast_fusion), channel_id=1, source_target_pairs={{32,0},{40,8},{48,16},{56,24},{0,32},{8,40},{16,48},{24,56},{33,1}... | collective-permute-start | bytes 884744 | tf_op jit(solution)/shard_map/ppermute | solution.py:35
  59.0 13.5 %collective-permute-done = bf16[1,288,512]{2,1,0:T(8,128)(2,1)S(1)} collective-permute-done((bf16[1,288,512]{2,1,0:T(8,128)(2,1)S(1)}, bf16[1,288,512]{2,1,0:T(8,128)(2,1)S(1)}, u32[]{:S(2)}, u32[]{:S(2)}) %collective-permute-start) | collective-permute-done | bytes 294944 | tf_op jit(solution)/shard_map/ppermute | solution.py:35
  72.5 2.7 %collective-permute-done.1 = bf16[1,288,512]{2,1,0:T(8,128)(2,1)S(1)} collective-permute-done((bf16[1,288,512]{2,1,0:T(8,128)(2,1)S(1)}, bf16[1,288,512]{2,1,0:T(8,128)(2,1)S(1)}, u32[]{:S(2)}, u32[]{:S(2)}) %collective-permute-start.1) | collective-permute-done | bytes 294944 | tf_op jit(solution)/shard_map/ppermute | solution.py:35
  76.1 5.1 %collective-permute-start.2 = (bf16[2,288,512]{2,1,0:T(8,128)(2,1)}, bf16[2,288,512]{2,1,0:T(8,128)(2,1)S(1)}, u32[]{:S(2)}, u32[]{:S(2)}) collective-permute-start(bf16[2,288,512]{2,1,0:T(8,128)(2,1)} %get-tuple-element.14), channel_id=1, source_target_pairs={{8,0},{16,8},{24,16},{32,24},{40,32},{48,40},{56,48},{0,56},{9,1},... | collective-permute-start | bytes 1769480 | tf_op jit(solution)/shard_map/ppermute | solution.py:35
  82.0 11.3 %all-to-all-start.3 = ((bf16[16,8,512]{2,1,0:T(8,128)(2,1)}), bf16[16,8,512]{2,1,0:T(8,128)(2,1)S(1)}, u32[]{:S(2)}, u32[]{:S(2)}) async-start(bf16[16,8,512]{2,1,0:T(8,128)(2,1)} %pad_bitcast_fusion), calls=%async_computation.3 | async-start | bytes 262144 | tf_op jit(solution)/shard_map/all_to_all | solution.py:17
  94.8 1.9 collective-permute-start.3
  99.0 7.3 %all-to-all-done.3 = bf16[16,8,512]{2,1,0:T(8,128)(2,1)S(1)} async-done(((bf16[16,8,512]{2,1,0:T(8,128)(2,1)}), bf16[16,8,512]{2,1,0:T(8,128)(2,1)S(1)}, u32[]{:S(2)}, u32[]{:S(2)}) %all-to-all-start.3) | async-done | bytes 131104 | tf_op jit(solution)/shard_map/all_to_all | solution.py:17
  107.8 4.7 %all-to-all-start.4 = ((bf16[16,8,512]{2,1,0:T(8,128)(2,1)}), bf16[16,8,512]{2,1,0:T(8,128)(2,1)S(1)}, u32[]{:S(2)}, u32[]{:S(2)}) async-start(bf16[16,8,512]{2,1,0:T(8,128)(2,1)} %broadcast_in_dim.141), calls=%async_computation.4 | async-start | bytes 262144 | tf_op jit(solution)/shard_map/all_to_all | solution.py:17
  113.4 1.7 constant_dynamic-update-slice_fusion
  116.1 9.7 %all-to-all-done.4 = bf16[16,8,512]{2,1,0:T(8,128)(2,1)S(1)} async-done(((bf16[16,8,512]{2,1,0:T(8,128)(2,1)}), bf16[16,8,512]{2,1,0:T(8,128)(2,1)S(1)}, u32[]{:S(2)}, u32[]{:S(2)}) %all-to-all-start.4) | async-done | bytes 131104 | tf_op jit(solution)/shard_map/all_to_all | solution.py:17
  129.9 5.4 %all-to-all-start.5 = ((bf16[8,72,256]{2,1,0:T(8,128)(2,1)}), bf16[8,72,256]{2,1,0:T(8,128)(2,1)S(1)}, u32[]{:S(2)}, u32[]{:S(2)}) async-start(bf16[8,72,256]{2,1,0:T(8,128)(2,1)} %fusion.10), calls=%async_computation.5 | async-start | bytes 589824 | tf_op jit(solution)/shard_map/all_to_all | solution.py:17
  135.3 5.8 %all-to-all-done.5 = bf16[8,72,256]{2,1,0:T(8,128)(2,1)S(1)} async-done(((bf16[8,72,256]{2,1,0:T(8,128)(2,1)}), bf16[8,72,256]{2,1,0:T(8,128)(2,1)S(1)}, u32[]{:S(2)}, u32[]{:S(2)}) %all-to-all-start.5) | async-done | bytes 294944 | tf_op jit(solution)/shard_map/all_to_all | solution.py:17
  141.6 8.5 %all_to_all.50 = bf16[8,64,128]{2,1,0:T(8,128)(2,1)S(1)} all-to-all(bf16[8,64,128]{2,1,0:T(8,128)(2,1)S(1)} %broadcast_in_dim.145), channel_id=1, replica_groups=mesh['ra_0'=16,'ra_1'=8,'cb'=8] {'cb'}, dimensions={0} | all-to-all | bytes 262144 | tf_op jit(solution)/shard_map/all_to_all | solution.py:17
  152.2 3.9 %all-to-all-start.7 = ((bf16[16,4,512]{2,1,0:T(4,128)(2,1)}), bf16[16,4,512]{2,1,0:T(4,128)(2,1)S(1)}, u32[]{:S(2)}, u32[]{:S(2)}) async-start(bf16[16,4,512]{2,1,0:T(4,128)(2,1)} %reshape.78), calls=%async_computation.7 | async-start | bytes 131072 | tf_op jit(solution)/shard_map/all_to_all | solution.py:17
  156.1 12.7 %all-to-all-done.7 = bf16[16,4,512]{2,1,0:T(4,128)(2,1)S(1)} async-done(((bf16[16,4,512]{2,1,0:T(4,128)(2,1)}), bf16[16,4,512]{2,1,0:T(4,128)(2,1)S(1)}, u32[]{:S(2)}, u32[]{:S(2)}) %all-to-all-start.7) | async-done | bytes 65568 | tf_op jit(solution)/shard_map/all_to_all | solution.py:17
  168.9 15.6 %all_to_all.51 = bf16[16,4,512]{2,1,0:T(4,128)(2,1)S(1)} all-to-all(bf16[16,4,512]{2,1,0:T(4,128)(2,1)S(1)} %broadcast_in_dim.146), channel_id=1, replica_groups=mesh['ra_0'=16,'ra_1'=8,'cb'=8] {'ra_0'}, dimensions={0} | all-to-all | bytes 131072 | tf_op jit(solution)/shard_map/all_to_all | solution.py:17
  184.6 27.9 %all_to_all.52 = bf16[8,64,512]{2,1,0:T(8,128)(2,1)S(1)} all-to-all(bf16[8,64,512]{2,1,0:T(8,128)(2,1)S(1)} %broadcast_in_dim.148), channel_id=1, replica_groups=mesh['ra_0'=16,'ra_1'=8,'cb'=8] {'ra_1'}, dimensions={0} | all-to-all | bytes 1048576 | tf_op jit(solution)/shard_map/all_to_all | solution.py:17
  (105 shorter events, 25.5 us)
Async XLA Ops:
  4.0 19.0 %copy-start.3 = (f32[2,88]{1,0:T(2,128)S(1)}, f32[2,88]{1,0:T(2,128)}, u32[]{:S(2)}) copy-start(f32[2,88]{1,0:T(2,128)} %param.15) | copy-start | bytes 2116
  4.0 19.0 %copy-start.4 = (f32[2,88]{1,0:T(2,128)S(1)}, f32[2,88]{1,0:T(2,128)}, u32[]{:S(2)}) copy-start(f32[2,88]{1,0:T(2,128)} %param.14) | copy-start | bytes 2116
  4.1 19.0 %copy-start.5 = (f32[2,88]{1,0:T(2,128)S(1)}, f32[2,88]{1,0:T(2,128)}, u32[]{:S(2)}) copy-start(f32[2,88]{1,0:T(2,128)} %param.19) | copy-start | bytes 2116
  4.1 19.0 %copy-start.2 = (f32[2,3,88]{2,0,1:T(2,128)S(1)}, f32[2,3,88]{2,0,1:T(2,128)}, u32[]{:S(2)}) copy-start(f32[2,3,88]{2,0,1:T(2,128)} %param.18) | copy-start | bytes 6340
  4.1 19.1 %copy-start = (f32[2,88,512]{2,1,0:T(8,128)S(1)}, f32[2,88,512]{2,1,0:T(8,128)}, u32[]{:S(2)}) copy-start(f32[2,88,512]{2,1,0:T(8,128)} %param.13) | copy-start | bytes 1081348
  6.6 22.2 %all-to-all-start = ((bf16[8,72,256]{2,1,0:T(8,128)(2,1)}), bf16[8,72,256]{2,1,0:T(8,128)(2,1)S(1)}, u32[]{:S(2)}, u32[]{:S(2)}) async-start(bf16[8,72,256]{2,1,0:T(8,128)(2,1)} %maximum_maximum_fusion.1), calls=%async_computation | async-start | bytes 589824 | tf_op jit(solution)/shard_map/all_to_all | solution.py:17
  30.0 9.4 %all-to-all-start.1 = ((bf16[8,64,128]{2,1,0:T(8,128)(2,1)}), bf16[8,64,128]{2,1,0:T(8,128)(2,1)S(1)}, u32[]{:S(2)}, u32[]{:S(2)}) async-start(bf16[8,64,128]{2,1,0:T(8,128)(2,1)} %broadcast_in_dim.137), calls=%async_computation.1 | async-start | bytes 262144 | tf_op jit(solution)/shard_map/all_to_all | solution.py:17
  39.9 41.3 %copy-start.1 = (f32[2,512]{1,0:T(2,128)S(1)}, f32[2,512]{1,0:T(2,128)}, u32[]{:S(2)}) copy-start(f32[2,512]{1,0:T(2,128)} %param.16) | copy-start | bytes 12292
  40.9 40.3 %all-to-all-start.2 = ((bf16[8,72,512]{2,1,0:T(8,128)(2,1)}), bf16[8,72,512]{2,1,0:T(8,128)(2,1)S(1)}, u32[]{:S(2)}, u32[]{:S(2)}) async-start(bf16[8,72,512]{2,1,0:T(8,128)(2,1)} %maximum_maximum_fusion), calls=%async_computation.2 | async-start | bytes 1179648 | tf_op jit(solution)/shard_map/all_to_all | solution.py:17
  44.5 28.0 %collective-permute-start = (bf16[1,288,512]{2,1,0:T(8,128)(2,1)S(1)}, bf16[1,288,512]{2,1,0:T(8,128)(2,1)S(1)}, u32[]{:S(2)}, u32[]{:S(2)}) collective-permute-start(bf16[1,288,512]{2,1,0:T(8,128)(2,1)S(1)} %maximum_bitcast_fusion), channel_id=1, source_target_pairs={{16,0},{24,8},{32,16},{40,24},{48,32},{56,40},{0,48},{8,56},{17,1}... | collective-permute-start | bytes 884744 | tf_op jit(solution)/shard_map/ppermute | solution.py:35
  50.4 24.7 %collective-permute-start.1 = (bf16[1,288,512]{2,1,0:T(8,128)(2,1)S(1)}, bf16[1,288,512]{2,1,0:T(8,128)(2,1)S(1)}, u32[]{:S(2)}, u32[]{:S(2)}) collective-permute-start(bf16[1,288,512]{2,1,0:T(8,128)(2,1)S(1)} %maximum_bitcast_fusion), channel_id=1, source_target_pairs={{48,0},{56,8},{0,16},{8,24},{16,32},{24,40},{32,48},{40,56},{49,1}... | collective-permute-start | bytes 884744 | tf_op jit(solution)/shard_map/ppermute | solution.py:35
  52.4 61.0 %collective-permute-start.4 = (bf16[1,288,512]{2,1,0:T(8,128)(2,1)S(1)}, bf16[1,288,512]{2,1,0:T(8,128)(2,1)}, u32[]{:S(2)}, u32[]{:S(2)}) collective-permute-start(bf16[1,288,512]{2,1,0:T(8,128)(2,1)S(1)} %maximum_bitcast_fusion), channel_id=1, source_target_pairs={{32,0},{40,8},{48,16},{56,24},{0,32},{8,40},{16,48},{24,56},{33,1}... | collective-permute-start | bytes 884744 | tf_op jit(solution)/shard_map/ppermute | solution.py:35
  76.1 22.1 %collective-permute-start.2 = (bf16[2,288,512]{2,1,0:T(8,128)(2,1)}, bf16[2,288,512]{2,1,0:T(8,128)(2,1)S(1)}, u32[]{:S(2)}, u32[]{:S(2)}) collective-permute-start(bf16[2,288,512]{2,1,0:T(8,128)(2,1)} %get-tuple-element.14), channel_id=1, source_target_pairs={{8,0},{16,8},{24,16},{32,24},{40,32},{48,40},{56,48},{0,56},{9,1},... | collective-permute-start | bytes 1769480 | tf_op jit(solution)/shard_map/ppermute | solution.py:35
  82.0 24.4 %all-to-all-start.3 = ((bf16[16,8,512]{2,1,0:T(8,128)(2,1)}), bf16[16,8,512]{2,1,0:T(8,128)(2,1)S(1)}, u32[]{:S(2)}, u32[]{:S(2)}) async-start(bf16[16,8,512]{2,1,0:T(8,128)(2,1)} %pad_bitcast_fusion), calls=%async_computation.3 | async-start | bytes 262144 | tf_op jit(solution)/shard_map/all_to_all | solution.py:17
  94.8 17.7 %collective-permute-start.3 = (bf16[2,288,512]{2,1,0:T(8,128)(2,1)S(1)}, bf16[2,288,512]{2,1,0:T(8,128)(2,1)S(1)}, u32[]{:S(2)}, u32[]{:S(2)}) collective-permute-start(bf16[2,288,512]{2,1,0:T(8,128)(2,1)S(1)} %get-tuple-element.13), channel_id=1, source_target_pairs={{56,0},{0,8},{8,16},{16,24},{24,32},{32,40},{40,48},{48,56},{57,1}... | collective-permute-start | bytes 1769480 | tf_op jit(solution)/shard_map/ppermute | solution.py:35
  107.8 18.0 %all-to-all-start.4 = ((bf16[16,8,512]{2,1,0:T(8,128)(2,1)}), bf16[16,8,512]{2,1,0:T(8,128)(2,1)S(1)}, u32[]{:S(2)}, u32[]{:S(2)}) async-start(bf16[16,8,512]{2,1,0:T(8,128)(2,1)} %broadcast_in_dim.141), calls=%async_computation.4 | async-start | bytes 262144 | tf_op jit(solution)/shard_map/all_to_all | solution.py:17
  129.9 11.2 %all-to-all-start.5 = ((bf16[8,72,256]{2,1,0:T(8,128)(2,1)}), bf16[8,72,256]{2,1,0:T(8,128)(2,1)S(1)}, u32[]{:S(2)}, u32[]{:S(2)}) async-start(bf16[8,72,256]{2,1,0:T(8,128)(2,1)} %fusion.10), calls=%async_computation.5 | async-start | bytes 589824 | tf_op jit(solution)/shard_map/all_to_all | solution.py:17
  152.2 16.6 %all-to-all-start.7 = ((bf16[16,4,512]{2,1,0:T(4,128)(2,1)}), bf16[16,4,512]{2,1,0:T(4,128)(2,1)S(1)}, u32[]{:S(2)}, u32[]{:S(2)}) async-start(bf16[16,4,512]{2,1,0:T(4,128)(2,1)} %reshape.78), calls=%async_computation.7 | async-start | bytes 131072 | tf_op jit(solution)/shard_map/all_to_all | solution.py:17

commit v4 on v3

--- a/solution.py
+++ b/solution.py
@@ -1,6 +1,7 @@
 import jax
 import jax.numpy as jnp
 from jax import lax
+from jax.experimental import pallas as pl
 from jax.sharding import Mesh
 from jax.sharding import PartitionSpec as P
 
@@ -63,17 +64,58 @@
     return jnp.concatenate([first, second, third], axis=0).astype(jnp.bfloat16)
 
 
-def side_by_side(gate_weight, up_weight):
-    return jnp.concatenate(
-        [padded_to(gate_weight, LANES, 1), padded_to(up_weight, LANES, 1)], axis=1
-    ).astype(jnp.bfloat16)
-
-
 def with_squares(product, squares, hidden):
     high, low = split_in_two(squares)
     column = lax.broadcasted_iota(jnp.int32, product.shape, product.ndim - 1)
     product = jnp.where(column == hidden, high, product)
     return jnp.where(column == hidden + 1, low, product)
+
+
+def first_products(tokens, gain, gate_weight, up_weight, blocks):
+    length, width = tokens.shape
+    hidden = gate_weight.shape[1]
+    block = length // blocks
+
+    def kernel(tokens_ref, gain_ref, gate_ref, up_ref, out_ref):
+        wide = tokens_ref[...].astype(jnp.float32)
+        squares = jnp.sum(wide * wide, axis=1, keepdims=True)
+        operand = (wide * gain_ref[0:1]).astype(jnp.bfloat16)
+        rest = jnp.zeros((LANES - hidden, width), jnp.float32)
+        weight = jnp.concatenate([gate_ref[0], rest, up_ref[0], rest], axis=0).astype(jnp.bfloat16)
+        product = lax.dot_general(
+            operand, weight, (((1,), (1,)), ((), ())), preferred_element_type=jnp.float32
+        )
+        high = squares.astype(jnp.bfloat16).astype(jnp.float32)
+        column = lax.broadcasted_iota(jnp.int32, product.shape, 1)
+        product = jnp.where(column == hidden, high, product)
+        product = jnp.where(column == hidden + 1, squares - high, product)
+        row = lax.broadcasted_iota(jnp.int32, (TILE, 2 * LANES), 0)
+        nothing = jnp.zeros((TILE, 2 * LANES), jnp.float32)
+        for j in range(blocks):
+            start = j * block
+            edge = nothing
+            if j > 0:
+                edge = jnp.where(row == 0, product[start - 1 : start], edge)
+            if j < blocks - 1:
+                edge = jnp.where(row == 1, product[start + block : start + block + 1], edge)
+            out_ref[j] = jnp.concatenate([product[start : start + block], edge], axis=0).astype(
+                jnp.bfloat16
+            )
+
+    shape = (blocks, block + TILE, 2 * LANES)
+    weight_block = pl.BlockSpec((1, hidden, width), lambda i: (0, 0, 0))
+    return pl.pallas_call(
+        kernel,
+        grid=(1,),
+        in_specs=[
+            pl.BlockSpec((length, width), lambda i: (0, 0)),
+            pl.BlockSpec(gain.shape, lambda i: (0, 0)),
+            weight_block,
+            weight_block,
+        ],
+        out_specs=pl.BlockSpec(shape, lambda i: (0, 0, 0)),
+        out_shape=jax.ShapeDtypeStruct(shape, jnp.bfloat16),
+    )(tokens, gain, gate_weight, up_weight)
 
 
 def activated(total, features, hidden, params):
@@ -128,14 +170,14 @@
     packed = gathered_in_steps(packed[None], "ra_1")
 
     params_0 = own_params(conv_taps[0], conv_bias[0], gate_scale[0], up_scale[0])
-    wide = tokens.astype(f32)
-    squares = jnp.sum(wide * wide, axis=1, keepdims=True)
-    operand = (wide * norm_gain[0]).astype(bf16)
-    product = jnp.dot(
-        operand, side_by_side(gate_weight[0], up_weight[0]), preferred_element_type=f32
-    )
-    product = with_squares(product, squares, hidden).astype(bf16)
-    total = swapped(with_neighbours(product, blocks_c), "cb").astype(f32).sum(axis=0)
+    product = first_products(
+        tokens,
+        norm_gain,
+        jnp.swapaxes(gate_weight, 1, 2),
+        jnp.swapaxes(up_weight, 1, 2),
+        blocks_c,
+    )
+    total = swapped(product, "cb").astype(f32).sum(axis=0)
     inner = activated(total, features, hidden, params_0)
     inner = sent_to_all(inner, "cb").reshape(length, LANES)
     down_0 = padded_to(down_weight[0], LANES, 0).astype(bf16)

time: 215 us -> 214 us (level)
  waiting for transfers between devices: 61.3 us -> 55.9 us
  local copies, waits for them, and re-layouts: 11.6 us -> 16.2 us
  Pallas kernels: 0 us -> 2.25 us
  other arithmetic: 9.53 us -> 7.31 us
    all_to_all x7, waiting for transfers between devices: 45.1 us -> 40.7 us  [swapped(): return lax.all_to_all(pieces, axes, 0, 0, tiled=True)]
    pallas_call x0 -> x1, Pallas kernels: none -> 2.25 us  [first_products(): pl.pallas_call(kernel, grid=(1,), in_specs=[pl.BlockSpec((length, width),...]
  transfers between devices with their start and end apart: 12 -> 12, of which waited for: 8 -> 8; matrix products, arithmetic and copies ran while one was open for 5% -> 9% of each run, Pallas kernels for 0% -> 0%
where the time goes in v4:
time: 214 us; the launch traced here: 212 us
  starting transfers between devices  73.6 us (34%)
  waiting for transfers between devices  55.9 us (26%)
  blocking collectives  51.9 us (24%)
  local copies, waits for them, and re-layouts  16.2 us (8%)
  other arithmetic  7.31 us (3%)
  matrix products  4.7 us (2%)
  Pallas kernels  2.25 us (1%)
    all_to_all x3, blocking collectives, swapped(): return lax.all_to_all(pieces, axes, 0, 0, tiled=True)  51.9 us
    all_to_all x7, starting transfers between devices, swapped(): return lax.all_to_all(pieces, axes, 0, 0, tiled=True)  51.8 us
    all_to_all x7, waiting for transfers between devices, swapped(): return lax.all_to_all(pieces, axes, 0, 0, tiled=True)  40.7 us
    ppermute x5, starting transfers between devices, taken_from(): lax.ppermute(value, axis, [((i + away) % size, i) for i in range(size)])  21.8 us
    ppermute x5, waiting for transfers between devices, taken_from(): lax.ppermute(value, axis, [((i + away) % size, i) for i in range(size)])  15.2 us
  transfers between devices with their start and end apart: 12, of which 8 were waited for; matrix products, arithmetic and copies ran while one was open for 9% of the time, Pallas kernels for 0%

profile of v4, /device:TPU:6, one launch (start us, length us, event | category | flops | bytes accessed | tf_op | source)
XLA Modules:
  0.0 212.3 jit_solution(418079469476532777)
XLA Ops:
  0.0 2.2 %shard_map.100 = bf16[8,72,256]{2,1,0:T(8,128)(2,1)} custom-call(bf16[512,512]{1,0:T(8,128)(2,1)} %tokens_ref.1, f32[2,512]{1,0:T(2,128)} %gain_ref.1, f32[2,88,512]{2,1,0:T(8,128)} %bitcast.92, f32[2,88,512]{2,1,0:T(8,128)} %bitcast.93), custom_call_target="tpu_custom_call" | custom-call | tf_op jit(solution)/shard_map/pallas_call | solution.py:107
  2.3 16.5 %all-to-all-start = ((bf16[8,72,256]{2,1,0:T(8,128)(2,1)}), bf16[8,72,256]{2,1,0:T(8,128)(2,1)S(1)}, u32[]{:S(2)}, u32[]{:S(2)}) async-start(bf16[8,72,256]{2,1,0:T(8,128)(2,1)} %shard_map.100), calls=%async_computation | async-start | bytes 589824 | tf_op jit(solution)/shard_map/all_to_all | solution.py:18
  21.8 2.6 %all-to-all-done = bf16[8,72,256]{2,1,0:T(8,128)(2,1)S(1)} async-done(((bf16[8,72,256]{2,1,0:T(8,128)(2,1)}), bf16[8,72,256]{2,1,0:T(8,128)(2,1)S(1)}, u32[]{:S(2)}, u32[]{:S(2)}) %all-to-all-start) | async-done | bytes 294944 | tf_op jit(solution)/shard_map/all_to_all | solution.py:18
  25.7 5.4 %all-to-all-start.1 = ((bf16[8,64,128]{2,1,0:T(8,128)(2,1)}), bf16[8,64,128]{2,1,0:T(8,128)(2,1)S(1)}, u32[]{:S(2)}, u32[]{:S(2)}) async-start(bf16[8,64,128]{2,1,0:T(8,128)(2,1)} %broadcast_in_dim.108), calls=%async_computation.1 | async-start | bytes 262144 | tf_op jit(solution)/shard_map/all_to_all | solution.py:18
  31.2 3.9 %all-to-all-done.1 = bf16[8,64,128]{2,1,0:T(8,128)(2,1)S(1)} async-done(((bf16[8,64,128]{2,1,0:T(8,128)(2,1)}), bf16[8,64,128]{2,1,0:T(8,128)(2,1)S(1)}, u32[]{:S(2)}, u32[]{:S(2)}) %all-to-all-start.1) | async-done | bytes 131104 | tf_op jit(solution)/shard_map/all_to_all | solution.py:18
  36.5 3.5 %all-to-all-start.2 = ((bf16[8,72,512]{2,1,0:T(8,128)(2,1)}), bf16[8,72,512]{2,1,0:T(8,128)(2,1)S(1)}, u32[]{:S(2)}, u32[]{:S(2)}) async-start(bf16[8,72,512]{2,1,0:T(8,128)(2,1)} %maximum_maximum_fusion), calls=%async_computation.2 | async-start | bytes 1179648 | tf_op jit(solution)/shard_map/all_to_all | solution.py:18
  41.2 6.0 %collective-permute-start = (bf16[1,288,512]{2,1,0:T(8,128)(2,1)S(1)}, bf16[1,288,512]{2,1,0:T(8,128)(2,1)S(1)}, u32[]{:S(2)}, u32[]{:S(2)}) collective-permute-start(bf16[1,288,512]{2,1,0:T(8,128)(2,1)S(1)} %maximum_bitcast_fusion), channel_id=1, source_target_pairs={{16,0},{24,8},{32,16},{40,24},{48,32},{56,40},{0,48},{8,56},{17,1}... | collective-permute-start | bytes 884744 | tf_op jit(solution)/shard_map/ppermute | solution.py:36
  47.1 1.9 collective-permute-start.1
  49.1 6.6 %collective-permute-start.4 = (bf16[1,288,512]{2,1,0:T(8,128)(2,1)S(1)}, bf16[1,288,512]{2,1,0:T(8,128)(2,1)}, u32[]{:S(2)}, u32[]{:S(2)}) collective-permute-start(bf16[1,288,512]{2,1,0:T(8,128)(2,1)S(1)} %maximum_bitcast_fusion), channel_id=1, source_target_pairs={{32,0},{40,8},{48,16},{56,24},{0,32},{8,40},{16,48},{24,56},{33,1}... | collective-permute-start | bytes 884744 | tf_op jit(solution)/shard_map/ppermute | solution.py:36
  55.7 12.4 %collective-permute-done = bf16[1,288,512]{2,1,0:T(8,128)(2,1)S(1)} collective-permute-done((bf16[1,288,512]{2,1,0:T(8,128)(2,1)S(1)}, bf16[1,288,512]{2,1,0:T(8,128)(2,1)S(1)}, u32[]{:S(2)}, u32[]{:S(2)}) %collective-permute-start) | collective-permute-done | bytes 294944 | tf_op jit(solution)/shard_map/ppermute | solution.py:36
  68.1 2.8 %collective-permute-done.1 = bf16[1,288,512]{2,1,0:T(8,128)(2,1)S(1)} collective-permute-done((bf16[1,288,512]{2,1,0:T(8,128)(2,1)S(1)}, bf16[1,288,512]{2,1,0:T(8,128)(2,1)S(1)}, u32[]{:S(2)}, u32[]{:S(2)}) %collective-permute-start.1) | collective-permute-done | bytes 294944 | tf_op jit(solution)/shard_map/ppermute | solution.py:36
  71.0 5.3 %collective-permute-start.2 = (bf16[2,288,512]{2,1,0:T(8,128)(2,1)S(1)}, bf16[2,288,512]{2,1,0:T(8,128)(2,1)S(1)}, u32[]{:S(2)}, u32[]{:S(2)}) collective-permute-start(bf16[2,288,512]{2,1,0:T(8,128)(2,1)S(1)} %get-tuple-element.14), channel_id=1, source_target_pairs={{8,0},{16,8},{24,16},{32,24},{40,32},{48,40},{56,48},{0,56},{9,1},... | collective-permute-start | bytes 1769480 | tf_op jit(solution)/shard_map/ppermute | solution.py:36
  79.2 11.0 %all-to-all-start.3 = ((bf16[16,8,512]{2,1,0:T(8,128)(2,1)}), bf16[16,8,512]{2,1,0:T(8,128)(2,1)}, u32[]{:S(2)}, u32[]{:S(2)}) async-start(bf16[16,8,512]{2,1,0:T(8,128)(2,1)} %pad_bitcast_fusion), calls=%async_computation.3 | async-start | bytes 262144 | tf_op jit(solution)/shard_map/all_to_all | solution.py:18
  92.8 2.0 collective-permute-start.3
  97.2 6.2 %all-to-all-done.3 = bf16[16,8,512]{2,1,0:T(8,128)(2,1)} async-done(((bf16[16,8,512]{2,1,0:T(8,128)(2,1)}), bf16[16,8,512]{2,1,0:T(8,128)(2,1)}, u32[]{:S(2)}, u32[]{:S(2)}) %all-to-all-start.3) | async-done | bytes 131104 | tf_op jit(solution)/shard_map/all_to_all | solution.py:18
  105.8 5.8 %all-to-all-start.4 = ((bf16[16,8,512]{2,1,0:T(8,128)(2,1)}), bf16[16,8,512]{2,1,0:T(8,128)(2,1)S(1)}, u32[]{:S(2)}, u32[]{:S(2)}) async-start(bf16[16,8,512]{2,1,0:T(8,128)(2,1)} %broadcast_in_dim.112), calls=%async_computation.4 | async-start | bytes 262144 | tf_op jit(solution)/shard_map/all_to_all | solution.py:18
  115.2 9.5 %all-to-all-done.4 = bf16[16,8,512]{2,1,0:T(8,128)(2,1)S(1)} async-done(((bf16[16,8,512]{2,1,0:T(8,128)(2,1)}), bf16[16,8,512]{2,1,0:T(8,128)(2,1)S(1)}, u32[]{:S(2)}, u32[]{:S(2)}) %all-to-all-start.4) | async-done | bytes 131104 | tf_op jit(solution)/shard_map/all_to_all | solution.py:18
  128.8 5.5 %all-to-all-start.5 = ((bf16[8,72,256]{2,1,0:T(8,128)(2,1)}), bf16[8,72,256]{2,1,0:T(8,128)(2,1)S(1)}, u32[]{:S(2)}, u32[]{:S(2)}) async-start(bf16[8,72,256]{2,1,0:T(8,128)(2,1)} %fusion.6), calls=%async_computation.5 | async-start | bytes 589824 | tf_op jit(solution)/shard_map/all_to_all | solution.py:18
  134.2 5.8 %all-to-all-done.5 = bf16[8,72,256]{2,1,0:T(8,128)(2,1)S(1)} async-done(((bf16[8,72,256]{2,1,0:T(8,128)(2,1)}), bf16[8,72,256]{2,1,0:T(8,128)(2,1)S(1)}, u32[]{:S(2)}, u32[]{:S(2)}) %all-to-all-start.5) | async-done | bytes 294944 | tf_op jit(solution)/shard_map/all_to_all | solution.py:18
  140.6 8.5 %all_to_all.50 = bf16[8,64,128]{2,1,0:T(8,128)(2,1)S(1)} all-to-all(bf16[8,64,128]{2,1,0:T(8,128)(2,1)S(1)} %broadcast_in_dim.116), channel_id=1, replica_groups=mesh['ra_0'=16,'ra_1'=8,'cb'=8] {'cb'}, dimensions={0} | all-to-all | bytes 262144 | tf_op jit(solution)/shard_map/all_to_all | solution.py:18
  151.1 4.0 %all-to-all-start.7 = ((bf16[16,4,512]{2,1,0:T(4,128)(2,1)}), bf16[16,4,512]{2,1,0:T(4,128)(2,1)S(1)}, u32[]{:S(2)}, u32[]{:S(2)}) async-start(bf16[16,4,512]{2,1,0:T(4,128)(2,1)} %reshape.66), calls=%async_computation.7 | async-start | bytes 131072 | tf_op jit(solution)/shard_map/all_to_all | solution.py:18
  155.2 12.7 %all-to-all-done.7 = bf16[16,4,512]{2,1,0:T(4,128)(2,1)S(1)} async-done(((bf16[16,4,512]{2,1,0:T(4,128)(2,1)}), bf16[16,4,512]{2,1,0:T(4,128)(2,1)S(1)}, u32[]{:S(2)}, u32[]{:S(2)}) %all-to-all-start.7) | async-done | bytes 65568 | tf_op jit(solution)/shard_map/all_to_all | solution.py:18
  168.0 15.6 %all_to_all.51 = bf16[16,4,512]{2,1,0:T(4,128)(2,1)S(1)} all-to-all(bf16[16,4,512]{2,1,0:T(4,128)(2,1)S(1)} %broadcast_in_dim.117), channel_id=1, replica_groups=mesh['ra_0'=16,'ra_1'=8,'cb'=8] {'ra_0'}, dimensions={0} | all-to-all | bytes 131072 | tf_op jit(solution)/shard_map/all_to_all | solution.py:18
  183.7 27.8 %all_to_all.52 = bf16[8,64,512]{2,1,0:T(8,128)(2,1)S(1)} all-to-all(bf16[8,64,512]{2,1,0:T(8,128)(2,1)S(1)} %broadcast_in_dim.119), channel_id=1, replica_groups=mesh['ra_0'=16,'ra_1'=8,'cb'=8] {'ra_1'}, dimensions={0} | all-to-all | bytes 1048576 | tf_op jit(solution)/shard_map/all_to_all | solution.py:18
  (97 shorter events, 28.2 us)
Async XLA Ops:
  0.0 21.8 %copy-start = (f32[2,88,512]{2,1,0:T(8,128)S(1)}, f32[2,88,512]{2,1,0:T(8,128)}, u32[]{:S(2)}) copy-start(f32[2,88,512]{2,1,0:T(8,128)} %param.13) | copy-start | bytes 1081348
  2.3 22.2 %all-to-all-start = ((bf16[8,72,256]{2,1,0:T(8,128)(2,1)}), bf16[8,72,256]{2,1,0:T(8,128)(2,1)S(1)}, u32[]{:S(2)}, u32[]{:S(2)}) async-start(bf16[8,72,256]{2,1,0:T(8,128)(2,1)} %shard_map.100), calls=%async_computation | async-start | bytes 589824 | tf_op jit(solution)/shard_map/all_to_all | solution.py:18
  25.7 9.4 %all-to-all-start.1 = ((bf16[8,64,128]{2,1,0:T(8,128)(2,1)}), bf16[8,64,128]{2,1,0:T(8,128)(2,1)S(1)}, u32[]{:S(2)}, u32[]{:S(2)}) async-start(bf16[8,64,128]{2,1,0:T(8,128)(2,1)} %broadcast_in_dim.108), calls=%async_computation.1 | async-start | bytes 262144 | tf_op jit(solution)/shard_map/all_to_all | solution.py:18
  31.1 24.6 %copy-start.2 = (f32[2,512]{1,0:T(2,128)S(1)}, f32[2,512]{1,0:T(2,128)}, u32[]{:S(2)}) copy-start(f32[2,512]{1,0:T(2,128)} %param.16) | copy-start | bytes 12292
  36.5 40.4 %all-to-all-start.2 = ((bf16[8,72,512]{2,1,0:T(8,128)(2,1)}), bf16[8,72,512]{2,1,0:T(8,128)(2,1)S(1)}, u32[]{:S(2)}, u32[]{:S(2)}) async-start(bf16[8,72,512]{2,1,0:T(8,128)(2,1)} %maximum_maximum_fusion), calls=%async_computation.2 | async-start | bytes 1179648 | tf_op jit(solution)/shard_map/all_to_all | solution.py:18
  40.1 50.7 %copy-start.1 = (f32[2,512]{1,0:T(2,128)S(1)}, f32[2,512]{1,0:T(2,128)}, u32[]{:S(2)}) copy-start(f32[2,512]{1,0:T(2,128)} %gain_ref.1) | copy-start | bytes 12292
  41.2 27.0 %collective-permute-start = (bf16[1,288,512]{2,1,0:T(8,128)(2,1)S(1)}, bf16[1,288,512]{2,1,0:T(8,128)(2,1)S(1)}, u32[]{:S(2)}, u32[]{:S(2)}) collective-permute-start(bf16[1,288,512]{2,1,0:T(8,128)(2,1)S(1)} %maximum_bitcast_fusion), channel_id=1, source_target_pairs={{16,0},{24,8},{32,16},{40,24},{48,32},{56,40},{0,48},{8,56},{17,1}... | collective-permute-start | bytes 884744 | tf_op jit(solution)/shard_map/ppermute | solution.py:36
  47.1 23.7 %collective-permute-start.1 = (bf16[1,288,512]{2,1,0:T(8,128)(2,1)S(1)}, bf16[1,288,512]{2,1,0:T(8,128)(2,1)S(1)}, u32[]{:S(2)}, u32[]{:S(2)}) collective-permute-start(bf16[1,288,512]{2,1,0:T(8,128)(2,1)S(1)} %maximum_bitcast_fusion), channel_id=1, source_target_pairs={{48,0},{56,8},{0,16},{8,24},{16,32},{24,40},{32,48},{40,56},{49,1}... | collective-permute-start | bytes 884744 | tf_op jit(solution)/shard_map/ppermute | solution.py:36
  49.1 63.4 %collective-permute-start.4 = (bf16[1,288,512]{2,1,0:T(8,128)(2,1)S(1)}, bf16[1,288,512]{2,1,0:T(8,128)(2,1)}, u32[]{:S(2)}, u32[]{:S(2)}) collective-permute-start(bf16[1,288,512]{2,1,0:T(8,128)(2,1)S(1)} %maximum_bitcast_fusion), channel_id=1, source_target_pairs={{32,0},{40,8},{48,16},{56,24},{0,32},{8,40},{16,48},{24,56},{33,1}... | collective-permute-start | bytes 884744 | tf_op jit(solution)/shard_map/ppermute | solution.py:36
  71.0 25.3 %collective-permute-start.2 = (bf16[2,288,512]{2,1,0:T(8,128)(2,1)S(1)}, bf16[2,288,512]{2,1,0:T(8,128)(2,1)S(1)}, u32[]{:S(2)}, u32[]{:S(2)}) collective-permute-start(bf16[2,288,512]{2,1,0:T(8,128)(2,1)S(1)} %get-tuple-element.14), channel_id=1, source_target_pairs={{8,0},{16,8},{24,16},{32,24},{40,32},{48,40},{56,48},{0,56},{9,1},... | collective-permute-start | bytes 1769480 | tf_op jit(solution)/shard_map/ppermute | solution.py:36
  79.2 24.2 %all-to-all-start.3 = ((bf16[16,8,512]{2,1,0:T(8,128)(2,1)}), bf16[16,8,512]{2,1,0:T(8,128)(2,1)}, u32[]{:S(2)}, u32[]{:S(2)}) async-start(bf16[16,8,512]{2,1,0:T(8,128)(2,1)} %pad_bitcast_fusion), calls=%async_computation.3 | async-start | bytes 262144 | tf_op jit(solution)/shard_map/all_to_all | solution.py:18
  92.8 11.5 %copy-start.3 = (pred[8]{0:T(512)(128)(4,1)S(1)}, pred[8]{0:T(512)(128)(4,1)}, u32[]{:S(2)}) copy-start(pred[8]{0:T(512)(128)(4,1)} %get-tuple-element.54) | copy-start | bytes 28
  92.8 11.5 %copy-start.4 = (pred[8]{0:T(512)(128)(4,1)S(1)}, pred[8]{0:T(512)(128)(4,1)}, u32[]{:S(2)}) copy-start(pred[8]{0:T(512)(128)(4,1)} %get-tuple-element.55) | copy-start | bytes 28
  92.8 18.8 %collective-permute-start.3 = (bf16[2,288,512]{2,1,0:T(8,128)(2,1)S(1)}, bf16[2,288,512]{2,1,0:T(8,128)(2,1)S(1)}, u32[]{:S(2)}, u32[]{:S(2)}) collective-permute-start(bf16[2,288,512]{2,1,0:T(8,128)(2,1)S(1)} %get-tuple-element.13), channel_id=1, source_target_pairs={{56,0},{0,8},{8,16},{16,24},{24,32},{32,40},{40,48},{48,56},{57,1}... | collective-permute-start | bytes 1769480 | tf_op jit(solution)/shard_map/ppermute | solution.py:36
  95.6 29.3 %copy-start.5 = (f32[1,512]{1,0:T(1,128)S(1)}, f32[1,512]{1,0:T(1,128)}, u32[]{:S(2)}) copy-start(f32[1,512]{1,0:T(1,128)} %slice.227) | copy-start | bytes 6148
  105.8 18.9 %all-to-all-start.4 = ((bf16[16,8,512]{2,1,0:T(8,128)(2,1)}), bf16[16,8,512]{2,1,0:T(8,128)(2,1)S(1)}, u32[]{:S(2)}, u32[]{:S(2)}) async-start(bf16[16,8,512]{2,1,0:T(8,128)(2,1)} %broadcast_in_dim.112), calls=%async_computation.4 | async-start | bytes 262144 | tf_op jit(solution)/shard_map/all_to_all | solution.py:18
  111.6 16.3 %copy-start.6 = (pred[256]{0:T(512)(128)(4,1)S(1)}, pred[256]{0:T(512)(128)(4,1)}, u32[]{:S(2)}) copy-start(pred[256]{0:T(512)(128)(4,1)} %get-tuple-element.58) | copy-start | bytes 772
  111.6 16.3 %copy-start.7 = (pred[256]{0:T(512)(128)(4,1)S(1)}, pred[256]{0:T(512)(128)(4,1)}, u32[]{:S(2)}) copy-start(pred[256]{0:T(512)(128)(4,1)} %get-tuple-element.59) | copy-start | bytes 772
  128.8 11.2 %all-to-all-start.5 = ((bf16[8,72,256]{2,1,0:T(8,128)(2,1)}), bf16[8,72,256]{2,1,0:T(8,128)(2,1)S(1)}, u32[]{:S(2)}, u32[]{:S(2)}) async-start(bf16[8,72,256]{2,1,0:T(8,128)(2,1)} %fusion.6), calls=%async_computation.5 | async-start | bytes 589824 | tf_op jit(solution)/shard_map/all_to_all | solution.py:18
  151.1 16.8 %all-to-all-start.7 = ((bf16[16,4,512]{2,1,0:T(4,128)(2,1)}), bf16[16,4,512]{2,1,0:T(4,128)(2,1)S(1)}, u32[]{:S(2)}, u32[]{:S(2)}) async-start(bf16[16,4,512]{2,1,0:T(4,128)(2,1)} %reshape.66), calls=%async_computation.7 | async-start | bytes 131072 | tf_op jit(solution)/shard_map/all_to_all | solution.py:18

commit v5 on v4

--- a/solution.py
+++ b/solution.py
@@ -40,7 +40,7 @@
     behind = taken_from(own, -2)
     odd_ahead = taken_from(jnp.concatenate([own, ahead]), 1)
     odd_behind = taken_from(jnp.concatenate([own, behind]), -1)
-    return jnp.concatenate([own, ahead, behind, odd_ahead, odd_behind, far])
+    return jnp.concatenate([own, ahead, behind, far, odd_ahead, odd_behind])
 
 
 def with_neighbours(rows, blocks):
@@ -182,22 +182,38 @@
     inner = sent_to_all(inner, "cb").reshape(length, LANES)
     down_0 = padded_to(down_weight[0], LANES, 0).astype(bf16)
     term = jnp.dot(inner, down_0, preferred_element_type=f32).astype(bf16)
-    part = swapped(with_neighbours(term, blocks_y), "ra_1").astype(f32).sum(axis=0)
-    share_rows = TILE
-    part = padded_to(part.astype(bf16), share_rows * blocks_z, 0)
-    part = swapped(part.reshape(blocks_z, share_rows, width), "ra_0").astype(f32).sum(axis=0)
-
-    start = block * at_y
-    mains = block // share_rows
-    own = lax.dynamic_slice_in_dim(tokens, start + share_rows * jnp.minimum(at_z, mains - 1), share_rows, 0)
-    before = lax.dynamic_slice_in_dim(tokens, jnp.maximum(start - 1, 0), 1, 0)
-    after = lax.dynamic_slice_in_dim(tokens, jnp.minimum(start + block, length - 1), 1, 0)
-    row = lax.broadcasted_iota(jnp.int32, (share_rows, 1), 0)
-    edge = jnp.where((row == 0) & (at_y > 0), before, jnp.zeros_like(before))
-    edge = jnp.where((row == 1) & (at_y < blocks_y - 1), after, edge)
-    own = jnp.where(at_z < mains, own, jnp.where(at_z == mains, edge, jnp.zeros_like(edge)))
-    fresh = (residual_scale * own.astype(f32) + part * down_scale[0]).astype(bf16)
-    hstate = sent_to_all(fresh, "ra_0").reshape(blocks_z * share_rows, width)[: block + TILE]
+
+    halves = 2
+    groups = blocks_z // halves
+    share_rows, half = block // groups, width // halves
+    term = term.reshape(blocks_y, groups, share_rows, halves, half).transpose(1, 3, 0, 2, 4)
+    part = swapped(term.reshape(blocks_z, blocks_y * share_rows, half), "ra_0")
+    part = part.astype(f32).sum(axis=0).astype(bf16)
+    part = swapped(with_neighbours(part, blocks_y), "ra_1").astype(f32).sum(axis=0)
+    group, column = at_z // halves, (at_z % halves) * half
+
+    def residual_rows(block_at, row, count):
+        start = jnp.clip(block_at, 0, blocks_y - 1) * block + group * share_rows + row
+        rows = lax.dynamic_slice(tokens, (start, column), (count, half))
+        inside = (block_at >= 0) & (block_at < blocks_y)
+        return jnp.where(inside, rows, jnp.zeros_like(rows))
+
+    own = jnp.concatenate(
+        [
+            residual_rows(at_y, 0, share_rows),
+            residual_rows(at_y - 1, share_rows - 1, 1),
+            residual_rows(at_y + 1, 0, 1),
+            jnp.zeros((TILE - 2, half), bf16),
+        ],
+        axis=0,
+    )
+    scale = lax.dynamic_slice_in_dim(down_scale[0], column, half, 0)
+    fresh = (residual_scale * own.astype(f32) + part * scale).astype(bf16)
+    fresh = sent_to_all(fresh, "ra_0").reshape(groups, halves, share_rows + TILE, half)
+    rows = fresh[:, :, :share_rows].transpose(0, 2, 1, 3).reshape(block, width)
+    before = fresh[groups - 1, :, share_rows].reshape(1, width)
+    after = fresh[0, :, share_rows + 1].reshape(1, width)
+    hstate = jnp.concatenate([rows, before, after, jnp.zeros((TILE - 2, width), bf16)], axis=0)
 
     wide = hstate.astype(f32)
     squares = jnp.sum(wide * wide, axis=1, keepdims=True)

time: 214 us -> 210 us (0.981)
  blocking collectives: 51.9 us -> 42.5 us
  starting transfers between devices: 73.6 us -> 79.5 us
  waiting for transfers between devices: 55.9 us -> 59.9 us
  local copies, waits for them, and re-layouts: 16.2 us -> 13.2 us
    all_to_all x3, blocking collectives: 51.9 us -> 42.5 us  [swapped(): return lax.all_to_all(pieces, axes, 0, 0, tiled=True)]
    all_to_all x7, starting transfers between devices: 51.8 us -> 59.2 us  [swapped(): return lax.all_to_all(pieces, axes, 0, 0, tiled=True)]
    all_to_all x7, waiting for transfers between devices: 40.7 us -> 46 us  [swapped(): return lax.all_to_all(pieces, axes, 0, 0, tiled=True)]
  transfers between devices with their start and end apart: 12 -> 12, of which waited for: 8 -> 7; matrix products, arithmetic and copies ran while one was open for 9% -> 7% of each run, Pallas kernels for 0% -> 0%
where the time goes in v5:
time: 210 us; the launch traced here: 208 us
  starting transfers between devices  79.5 us (38%)
  waiting for transfers between devices  59.9 us (29%)
  blocking collectives  42.5 us (20%)
  local copies, waits for them, and re-layouts  13.2 us (6%)
  other arithmetic  5.99 us (3%)
  matrix products  4.7 us (2%)
  Pallas kernels  2.25 us (1%)
    all_to_all x7, starting transfers between devices, swapped(): return lax.all_to_all(pieces, axes, 0, 0, tiled=True)  59.2 us
    all_to_all x7, waiting for transfers between devices, swapped(): return lax.all_to_all(pieces, axes, 0, 0, tiled=True)  46 us
    all_to_all x3, blocking collectives, swapped(): return lax.all_to_all(pieces, axes, 0, 0, tiled=True)  42.5 us
    ppermute x5, starting transfers between devices, taken_from(): lax.ppermute(value, axis, [((i + away) % size, i) for i in range(size)])  20.3 us
    ppermute x5, waiting for transfers between devices, taken_from(): lax.ppermute(value, axis, [((i + away) % size, i) for i in range(size)])  14 us
  transfers between devices with their start and end apart: 12, of which 7 were waited for; matrix products, arithmetic and copies ran while one was open for 7% of the time, Pallas kernels for 0%

profile of v5, /device:TPU:6, one launch (start us, length us, event | category | flops | bytes accessed | tf_op | source)
XLA Modules:
  0.0 208.5 jit_solution(17207354288288391428)
XLA Ops:
  0.0 2.2 %shard_map.100 = bf16[8,72,256]{2,1,0:T(8,128)(2,1)} custom-call(bf16[512,512]{1,0:T(8,128)(2,1)} %tokens_ref.1, f32[2,512]{1,0:T(2,128)} %gain_ref.1, f32[2,88,512]{2,1,0:T(8,128)} %bitcast.91, f32[2,88,512]{2,1,0:T(8,128)} %bitcast.92), custom_call_target="tpu_custom_call" | custom-call | tf_op jit(solution)/shard_map/pallas_call | solution.py:107
  2.3 16.5 %all-to-all-start = ((bf16[8,72,256]{2,1,0:T(8,128)(2,1)}), bf16[8,72,256]{2,1,0:T(8,128)(2,1)S(1)}, u32[]{:S(2)}, u32[]{:S(2)}) async-start(bf16[8,72,256]{2,1,0:T(8,128)(2,1)} %shard_map.100), calls=%async_computation | async-start | bytes 589824 | tf_op jit(solution)/shard_map/all_to_all | solution.py:18
  21.8 2.7 %all-to-all-done = bf16[8,72,256]{2,1,0:T(8,128)(2,1)S(1)} async-done(((bf16[8,72,256]{2,1,0:T(8,128)(2,1)}), bf16[8,72,256]{2,1,0:T(8,128)(2,1)S(1)}, u32[]{:S(2)}, u32[]{:S(2)}) %all-to-all-start) | async-done | bytes 294944 | tf_op jit(solution)/shard_map/all_to_all | solution.py:18
  25.7 5.4 %all-to-all-start.1 = ((bf16[8,64,128]{2,1,0:T(8,128)(2,1)}), bf16[8,64,128]{2,1,0:T(8,128)(2,1)S(1)}, u32[]{:S(2)}, u32[]{:S(2)}) async-start(bf16[8,64,128]{2,1,0:T(8,128)(2,1)} %broadcast_in_dim.68), calls=%async_computation.1 | async-start | bytes 262144 | tf_op jit(solution)/shard_map/all_to_all | solution.py:18
  31.1 4.0 %all-to-all-done.1 = bf16[8,64,128]{2,1,0:T(8,128)(2,1)S(1)} async-done(((bf16[8,64,128]{2,1,0:T(8,128)(2,1)}), bf16[8,64,128]{2,1,0:T(8,128)(2,1)S(1)}, u32[]{:S(2)}, u32[]{:S(2)}) %all-to-all-start.1) | async-done | bytes 131104 | tf_op jit(solution)/shard_map/all_to_all | solution.py:18
  36.3 7.2 %all-to-all-start.2 = ((bf16[16,64,256]{2,1,0:T(8,128)(2,1)}), bf16[16,64,256]{2,1,0:T(8,128)(2,1)S(1)}, u32[]{:S(2)}, u32[]{:S(2)}) async-start(bf16[16,64,256]{2,1,0:T(8,128)(2,1)} %bitcast.12), calls=%async_computation.2 | async-start | bytes 1048576 | tf_op jit(solution)/shard_map/all_to_all | solution.py:18
  44.6 6.2 %collective-permute-start = (bf16[1,288,512]{2,1,0:T(8,128)(2,1)S(1)}, bf16[1,288,512]{2,1,0:T(8,128)(2,1)S(1)}, u32[]{:S(2)}, u32[]{:S(2)}) collective-permute-start(bf16[1,288,512]{2,1,0:T(8,128)(2,1)S(1)} %maximum_bitcast_fusion), channel_id=1, source_target_pairs={{16,0},{24,8},{32,16},{40,24},{48,32},{56,40},{0,48},{8,56},{17,1}... | collective-permute-start | bytes 884744 | tf_op jit(solution)/shard_map/ppermute | solution.py:36
  50.7 1.9 collective-permute-start.1
  52.6 6.4 %collective-permute-start.2 = (bf16[1,288,512]{2,1,0:T(8,128)(2,1)S(1)}, bf16[1,288,512]{2,1,0:T(8,128)(2,1)S(1)}, u32[]{:S(2)}, u32[]{:S(2)}) collective-permute-start(bf16[1,288,512]{2,1,0:T(8,128)(2,1)S(1)} %maximum_bitcast_fusion), channel_id=1, source_target_pairs={{32,0},{40,8},{48,16},{56,24},{0,32},{8,40},{16,48},{24,56},{33,1}... | collective-permute-start | bytes 884744 | tf_op jit(solution)/shard_map/ppermute | solution.py:36
  61.5 13.9 %collective-permute-done = bf16[1,288,512]{2,1,0:T(8,128)(2,1)S(1)} collective-permute-done((bf16[1,288,512]{2,1,0:T(8,128)(2,1)S(1)}, bf16[1,288,512]{2,1,0:T(8,128)(2,1)S(1)}, u32[]{:S(2)}, u32[]{:S(2)}) %collective-permute-start) | collective-permute-done | bytes 294944 | tf_op jit(solution)/shard_map/ppermute | solution.py:36
  76.4 3.0 %collective-permute-start.3 = (bf16[2,288,512]{2,1,0:T(8,128)(2,1)}, bf16[2,288,512]{2,1,0:T(8,128)(2,1)S(1)}, u32[]{:S(2)}, u32[]{:S(2)}) collective-permute-start(bf16[2,288,512]{2,1,0:T(8,128)(2,1)} %get-tuple-element.14), channel_id=1, source_target_pairs={{8,0},{16,8},{24,16},{32,24},{40,32},{48,40},{56,48},{0,56},{9,1},... | collective-permute-start | bytes 1769480 | tf_op jit(solution)/shard_map/ppermute | solution.py:36
  79.4 2.8 %collective-permute-start.4 = (bf16[2,288,512]{2,1,0:T(8,128)(2,1)S(1)}, bf16[2,288,512]{2,1,0:T(8,128)(2,1)S(1)}, u32[]{:S(2)}, u32[]{:S(2)}) collective-permute-start(bf16[2,288,512]{2,1,0:T(8,128)(2,1)S(1)} %get-tuple-element.13), channel_id=1, source_target_pairs={{56,0},{0,8},{8,16},{16,24},{24,32},{32,40},{40,48},{48,56},{57,1}... | collective-permute-start | bytes 1769480 | tf_op jit(solution)/shard_map/ppermute | solution.py:36
  84.6 9.5 %all-to-all-start.3 = ((bf16[8,16,256]{2,1,0:T(8,128)(2,1)}), bf16[8,16,256]{2,1,0:T(8,128)(2,1)S(1)}, u32[]{:S(2)}, u32[]{:S(2)}) async-start(bf16[8,16,256]{2,1,0:T(8,128)(2,1)} %maximum_maximum_fusion.1), calls=%async_computation.3 | async-start | bytes 131072 | tf_op jit(solution)/shard_map/all_to_all | solution.py:18
  94.8 9.6 %all-to-all-done.3 = bf16[8,16,256]{2,1,0:T(8,128)(2,1)S(1)} async-done(((bf16[8,16,256]{2,1,0:T(8,128)(2,1)}), bf16[8,16,256]{2,1,0:T(8,128)(2,1)S(1)}, u32[]{:S(2)}, u32[]{:S(2)}) %all-to-all-start.3) | async-done | bytes 65568 | tf_op jit(solution)/shard_map/all_to_all | solution.py:18
  105.2 11.7 %all-to-all-start.4 = ((bf16[16,16,256]{2,1,0:T(8,128)(2,1)}), bf16[16,16,256]{2,1,0:T(8,128)(2,1)S(1)}, u32[]{:S(2)}, u32[]{:S(2)}) async-start(bf16[16,16,256]{2,1,0:T(8,128)(2,1)} %broadcast_in_dim.72), calls=%async_computation.4 | async-start | bytes 262144 | tf_op jit(solution)/shard_map/all_to_all | solution.py:18
  119.7 11.2 %all-to-all-done.4 = bf16[16,16,256]{2,1,0:T(8,128)(2,1)S(1)} async-done(((bf16[16,16,256]{2,1,0:T(8,128)(2,1)}), bf16[16,16,256]{2,1,0:T(8,128)(2,1)S(1)}, u32[]{:S(2)}, u32[]{:S(2)}) %all-to-all-start.4) | async-done | bytes 131104 | tf_op jit(solution)/shard_map/all_to_all | solution.py:18
  131.1 1.5 convolution_bitcast_fusion.1
  135.0 5.4 %all-to-all-start.5 = ((bf16[8,72,256]{2,1,0:T(8,128)(2,1)}), bf16[8,72,256]{2,1,0:T(8,128)(2,1)S(1)}, u32[]{:S(2)}, u32[]{:S(2)}) async-start(bf16[8,72,256]{2,1,0:T(8,128)(2,1)} %fusion.6), calls=%async_computation.5 | async-start | bytes 589824 | tf_op jit(solution)/shard_map/all_to_all | solution.py:18
  140.4 5.8 %all-to-all-done.5 = bf16[8,72,256]{2,1,0:T(8,128)(2,1)S(1)} async-done(((bf16[8,72,256]{2,1,0:T(8,128)(2,1)}), bf16[8,72,256]{2,1,0:T(8,128)(2,1)S(1)}, u32[]{:S(2)}, u32[]{:S(2)}) %all-to-all-start.5) | async-done | bytes 294944 | tf_op jit(solution)/shard_map/all_to_all | solution.py:18
  146.8 8.5 %all_to_all.50 = bf16[8,64,128]{2,1,0:T(8,128)(2,1)S(1)} all-to-all(bf16[8,64,128]{2,1,0:T(8,128)(2,1)S(1)} %broadcast_in_dim.77), channel_id=1, replica_groups=mesh['ra_0'=16,'ra_1'=8,'cb'=8] {'cb'}, dimensions={0} | all-to-all | bytes 262144 | tf_op jit(solution)/shard_map/all_to_all | solution.py:18
  157.3 3.5 %all-to-all-start.7 = ((bf16[16,4,512]{2,1,0:T(4,128)(2,1)}), bf16[16,4,512]{2,1,0:T(4,128)(2,1)S(1)}, u32[]{:S(2)}, u32[]{:S(2)}) async-start(bf16[16,4,512]{2,1,0:T(4,128)(2,1)} %reshape.102), calls=%async_computation.7 | async-start | bytes 131072 | tf_op jit(solution)/shard_map/all_to_all | solution.py:18
  160.8 12.8 %all-to-all-done.7 = bf16[16,4,512]{2,1,0:T(4,128)(2,1)S(1)} async-done(((bf16[16,4,512]{2,1,0:T(4,128)(2,1)}), bf16[16,4,512]{2,1,0:T(4,128)(2,1)S(1)}, u32[]{:S(2)}, u32[]{:S(2)}) %all-to-all-start.7) | async-done | bytes 65568 | tf_op jit(solution)/shard_map/all_to_all | solution.py:18
  173.7 15.5 %all_to_all.51 = bf16[16,4,512]{2,1,0:T(4,128)(2,1)S(1)} all-to-all(bf16[16,4,512]{2,1,0:T(4,128)(2,1)S(1)} %broadcast_in_dim.78), channel_id=1, replica_groups=mesh['ra_0'=16,'ra_1'=8,'cb'=8] {'ra_0'}, dimensions={0} | all-to-all | bytes 131072 | tf_op jit(solution)/shard_map/all_to_all | solution.py:18
  189.3 18.4 %all_to_all.52 = bf16[8,64,512]{2,1,0:T(8,128)(2,1)S(1)} all-to-all(bf16[8,64,512]{2,1,0:T(8,128)(2,1)S(1)} %broadcast_in_dim.80), channel_id=1, replica_groups=mesh['ra_0'=16,'ra_1'=8,'cb'=8] {'ra_1'}, dimensions={0} | all-to-all | bytes 1048576 | tf_op jit(solution)/shard_map/all_to_all | solution.py:18
  (89 shorter events, 22.4 us)
Async XLA Ops:
  0.0 21.8 %copy-start = (f32[2,88,512]{2,1,0:T(8,128)S(1)}, f32[2,88,512]{2,1,0:T(8,128)}, u32[]{:S(2)}) copy-start(f32[2,88,512]{2,1,0:T(8,128)} %param.13) | copy-start | bytes 1081348
  2.3 22.2 %all-to-all-start = ((bf16[8,72,256]{2,1,0:T(8,128)(2,1)}), bf16[8,72,256]{2,1,0:T(8,128)(2,1)S(1)}, u32[]{:S(2)}, u32[]{:S(2)}) async-start(bf16[8,72,256]{2,1,0:T(8,128)(2,1)} %shard_map.100), calls=%async_computation | async-start | bytes 589824 | tf_op jit(solution)/shard_map/all_to_all | solution.py:18
  25.0 34.2 %copy-start.1 = (f32[2,512]{1,0:T(2,128)S(1)}, f32[2,512]{1,0:T(2,128)}, u32[]{:S(2)}) copy-start(f32[2,512]{1,0:T(2,128)} %gain_ref.1) | copy-start | bytes 12292
  25.0 35.0 %copy-start.2 = (f32[2,512]{1,0:T(2,128)S(1)}, f32[2,512]{1,0:T(2,128)}, u32[]{:S(2)}) copy-start(f32[2,512]{1,0:T(2,128)} %param.16) | copy-start | bytes 12292
  25.7 9.4 %all-to-all-start.1 = ((bf16[8,64,128]{2,1,0:T(8,128)(2,1)}), bf16[8,64,128]{2,1,0:T(8,128)(2,1)S(1)}, u32[]{:S(2)}, u32[]{:S(2)}) async-start(bf16[8,64,128]{2,1,0:T(8,128)(2,1)} %broadcast_in_dim.68), calls=%async_computation.1 | async-start | bytes 262144 | tf_op jit(solution)/shard_map/all_to_all | solution.py:18
  36.3 47.5 %all-to-all-start.2 = ((bf16[16,64,256]{2,1,0:T(8,128)(2,1)}), bf16[16,64,256]{2,1,0:T(8,128)(2,1)S(1)}, u32[]{:S(2)}, u32[]{:S(2)}) async-start(bf16[16,64,256]{2,1,0:T(8,128)(2,1)} %bitcast.12), calls=%async_computation.2 | async-start | bytes 1048576 | tf_op jit(solution)/shard_map/all_to_all | solution.py:18
  44.6 30.9 %collective-permute-start = (bf16[1,288,512]{2,1,0:T(8,128)(2,1)S(1)}, bf16[1,288,512]{2,1,0:T(8,128)(2,1)S(1)}, u32[]{:S(2)}, u32[]{:S(2)}) collective-permute-start(bf16[1,288,512]{2,1,0:T(8,128)(2,1)S(1)} %maximum_bitcast_fusion), channel_id=1, source_target_pairs={{16,0},{24,8},{32,16},{40,24},{48,32},{56,40},{0,48},{8,56},{17,1}... | collective-permute-start | bytes 884744 | tf_op jit(solution)/shard_map/ppermute | solution.py:36
  50.7 24.8 %collective-permute-start.1 = (bf16[1,288,512]{2,1,0:T(8,128)(2,1)S(1)}, bf16[1,288,512]{2,1,0:T(8,128)(2,1)S(1)}, u32[]{:S(2)}, u32[]{:S(2)}) collective-permute-start(bf16[1,288,512]{2,1,0:T(8,128)(2,1)S(1)} %maximum_bitcast_fusion), channel_id=1, source_target_pairs={{48,0},{56,8},{0,16},{8,24},{16,32},{24,40},{32,48},{40,56},{49,1}... | collective-permute-start | bytes 884744 | tf_op jit(solution)/shard_map/ppermute | solution.py:36
  52.6 41.4 %collective-permute-start.2 = (bf16[1,288,512]{2,1,0:T(8,128)(2,1)S(1)}, bf16[1,288,512]{2,1,0:T(8,128)(2,1)S(1)}, u32[]{:S(2)}, u32[]{:S(2)}) collective-permute-start(bf16[1,288,512]{2,1,0:T(8,128)(2,1)S(1)} %maximum_bitcast_fusion), channel_id=1, source_target_pairs={{32,0},{40,8},{48,16},{56,24},{0,32},{8,40},{16,48},{24,56},{33,1}... | collective-permute-start | bytes 884744 | tf_op jit(solution)/shard_map/ppermute | solution.py:36
  76.4 40.5 %collective-permute-start.3 = (bf16[2,288,512]{2,1,0:T(8,128)(2,1)}, bf16[2,288,512]{2,1,0:T(8,128)(2,1)S(1)}, u32[]{:S(2)}, u32[]{:S(2)}) collective-permute-start(bf16[2,288,512]{2,1,0:T(8,128)(2,1)} %get-tuple-element.14), channel_id=1, source_target_pairs={{8,0},{16,8},{24,16},{32,24},{40,32},{48,40},{56,48},{0,56},{9,1},... | collective-permute-start | bytes 1769480 | tf_op jit(solution)/shard_map/ppermute | solution.py:36
  79.4 38.4 %collective-permute-start.4 = (bf16[2,288,512]{2,1,0:T(8,128)(2,1)S(1)}, bf16[2,288,512]{2,1,0:T(8,128)(2,1)S(1)}, u32[]{:S(2)}, u32[]{:S(2)}) collective-permute-start(bf16[2,288,512]{2,1,0:T(8,128)(2,1)S(1)} %get-tuple-element.13), channel_id=1, source_target_pairs={{56,0},{0,8},{8,16},{16,24},{24,32},{32,40},{40,48},{48,56},{57,1}... | collective-permute-start | bytes 1769480 | tf_op jit(solution)/shard_map/ppermute | solution.py:36
  84.6 19.8 %all-to-all-start.3 = ((bf16[8,16,256]{2,1,0:T(8,128)(2,1)}), bf16[8,16,256]{2,1,0:T(8,128)(2,1)S(1)}, u32[]{:S(2)}, u32[]{:S(2)}) async-start(bf16[8,16,256]{2,1,0:T(8,128)(2,1)} %maximum_maximum_fusion.1), calls=%async_computation.3 | async-start | bytes 131072 | tf_op jit(solution)/shard_map/all_to_all | solution.py:18
  105.2 25.7 %all-to-all-start.4 = ((bf16[16,16,256]{2,1,0:T(8,128)(2,1)}), bf16[16,16,256]{2,1,0:T(8,128)(2,1)S(1)}, u32[]{:S(2)}, u32[]{:S(2)}) async-start(bf16[16,16,256]{2,1,0:T(8,128)(2,1)} %broadcast_in_dim.72), calls=%async_computation.4 | async-start | bytes 262144 | tf_op jit(solution)/shard_map/all_to_all | solution.py:18
  135.0 11.2 %all-to-all-start.5 = ((bf16[8,72,256]{2,1,0:T(8,128)(2,1)}), bf16[8,72,256]{2,1,0:T(8,128)(2,1)S(1)}, u32[]{:S(2)}, u32[]{:S(2)}) async-start(bf16[8,72,256]{2,1,0:T(8,128)(2,1)} %fusion.6), calls=%async_computation.5 | async-start | bytes 589824 | tf_op jit(solution)/shard_map/all_to_all | solution.py:18
  157.3 16.3 %all-to-all-start.7 = ((bf16[16,4,512]{2,1,0:T(4,128)(2,1)}), bf16[16,4,512]{2,1,0:T(4,128)(2,1)S(1)}, u32[]{:S(2)}, u32[]{:S(2)}) async-start(bf16[16,4,512]{2,1,0:T(4,128)(2,1)} %reshape.102), calls=%async_computation.7 | async-start | bytes 131072 | tf_op jit(solution)/shard_map/all_to_all | solution.py:18

commit v6 on v5

--- a/solution.py
+++ b/solution.py
@@ -61,7 +61,7 @@
 def split_in_three(value):
     first, rest = split_in_two(value)
     second, third = split_in_two(rest)
-    return jnp.concatenate([first, second, third], axis=0).astype(jnp.bfloat16)
+    return tuple(part.astype(jnp.bfloat16) for part in (first, second, third))
 
 
 def with_squares(product, squares, hidden):
@@ -118,12 +118,12 @@
     )(tokens, gain, gate_weight, up_weight)
 
 
-def activated(total, features, hidden, params):
+def activated(total, features, hidden, up_at, params):
     rows = total.shape[0] - TILE
     square_sum = total[:, hidden : hidden + 1] + total[:, hidden + 1 : hidden + 2]
     rscale = lax.rsqrt(square_sum / features + norm_eps)
     gate = total[:, :LANES] * rscale * params[4]
-    upward = total[:rows, LANES:] * rscale[:rows] * params[5]
+    upward = total[:rows, up_at : up_at + LANES] * rscale[:rows] * params[5]
     main = gate[:rows]
     before = jnp.concatenate([gate[rows : rows + 1], main[:-1]], axis=0)
     after = jnp.concatenate([main[1:], gate[rows + 1 : rows + 2]], axis=0)
@@ -157,16 +157,20 @@
     f32, bf16 = jnp.float32, jnp.bfloat16
 
     params_1 = own_params(conv_taps[1], conv_bias[1], gate_scale[1], up_scale[1])
-    carried = padded_to(split_in_three(padded_to(params_1, TILE, 0)), width, 1)
+    carried = split_in_three(padded_to(padded_to(params_1, TILE, 0), width, 1))
     packed = jnp.concatenate(
         [
             gate_weight[1].T.astype(bf16),
+            carried[0],
             up_weight[1].T.astype(bf16),
+            carried[1],
+            carried[2],
             down_weight[1].astype(bf16),
-            carried,
         ],
         axis=0,
     )
+    up_at = hidden + TILE
+    down_at = 2 * hidden + 3 * TILE
     packed = gathered_in_steps(packed[None], "ra_1")
 
     params_0 = own_params(conv_taps[0], conv_bias[0], gate_scale[0], up_scale[0])
@@ -178,7 +182,7 @@
         blocks_c,
     )
     total = swapped(product, "cb").astype(f32).sum(axis=0)
-    inner = activated(total, features, hidden, params_0)
+    inner = activated(total, features, hidden, LANES, params_0)
     inner = sent_to_all(inner, "cb").reshape(length, LANES)
     down_0 = padded_to(down_weight[0], LANES, 0).astype(bf16)
     term = jnp.dot(inner, down_0, preferred_element_type=f32).astype(bf16)
@@ -218,23 +222,21 @@
     wide = hstate.astype(f32)
     squares = jnp.sum(wide * wide, axis=1, keepdims=True)
     operand = (wide * norm_gain[1]).astype(bf16)
-    product = jnp.concatenate(
-        [
-            padded_to(
-                jnp.einsum("td,ykd->ytk", operand, weight, preferred_element_type=f32), LANES, 2
-            )
-            for weight in (packed[:, :hidden], packed[:, hidden : 2 * hidden])
-        ],
-        axis=2,
+    product = jnp.einsum(
+        "td,ykd->ytk", operand, packed[:, : 2 * LANES], preferred_element_type=f32
     )
     product = with_squares(product, squares[None], hidden).astype(bf16)
     total = swapped(product, "cb").astype(f32).sum(axis=0)
     theirs = lax.dynamic_index_in_dim(packed, lax.axis_index("cb"), 0, keepdims=False)
-    theirs = theirs[3 * hidden :, :LANES].astype(f32).reshape(3, TILE, LANES)
-    theirs = theirs[0] + theirs[1] + theirs[2]
-    inner = activated(total, features, hidden, theirs)
+    theirs = theirs[:, :LANES].astype(f32)
+    theirs = (
+        theirs[hidden:up_at]
+        + theirs[down_at - 2 * TILE : down_at - TILE]
+        + theirs[down_at - TILE : down_at]
+    )
+    inner = activated(total, features, hidden, up_at, theirs)
     inner = sent_to_all(inner, "cb")
-    down_1 = packed[:, 2 * hidden : 3 * hidden]
+    down_1 = packed[:, down_at:]
     term = jnp.einsum("ytk,ykf->tf", inner[:, :, :hidden], down_1, preferred_element_type=f32)
     term = term.astype(bf16)
     share_rows = block // blocks_z

time: 210 us -> 210 us (level)
    unnamed x15 -> x18, local copies, waits for them, and re-layouts: 3.89 us -> 6.48 us
where the time goes in v6:
time: 210 us; the launch traced here: 208 us
  starting transfers between devices  79.5 us (38%)
  waiting for transfers between devices  59 us (28%)
  blocking collectives  42.5 us (20%)
  local copies, waits for them, and re-layouts  14.8 us (7%)
  matrix products  4.73 us (2%)
  other arithmetic  4.41 us (2%)
  Pallas kernels  2.25 us (1%)
    all_to_all x7, starting transfers between devices, swapped(): return lax.all_to_all(pieces, axes, 0, 0, tiled=True)  59.2 us
    all_to_all x7, waiting for transfers between devices, swapped(): return lax.all_to_all(pieces, axes, 0, 0, tiled=True)  45 us
    all_to_all x3, blocking collectives, swapped(): return lax.all_to_all(pieces, axes, 0, 0, tiled=True)  42.5 us
    ppermute x5, starting transfers between devices, taken_from(): lax.ppermute(value, axis, [((i + away) % size, i) for i in range(size)])  20.3 us
    ppermute x5, waiting for transfers between devices, taken_from(): lax.ppermute(value, axis, [((i + away) % size, i) for i in range(size)])  14 us
    unnamed x18, local copies, waits for them, and re-layouts  6.48 us
  transfers between devices with their start and end apart: 12, of which 7 were waited for; matrix products, arithmetic and copies ran while one was open for 7% of the time, Pallas kernels for 0%

profile of v6, /device:TPU:6, one launch (start us, length us, event | category | flops | bytes accessed | tf_op | source)
XLA Modules:
  0.0 207.5 jit_solution(4718554636799607230)
XLA Ops:
  0.0 2.2 %shard_map.100 = bf16[8,72,256]{2,1,0:T(8,128)(2,1)} custom-call(bf16[512,512]{1,0:T(8,128)(2,1)} %tokens_ref.1, f32[2,512]{1,0:T(2,128)} %gain_ref.1, f32[2,88,512]{2,1,0:T(8,128)} %bitcast.96, f32[2,88,512]{2,1,0:T(8,128)} %bitcast.97), custom_call_target="tpu_custom_call" | custom-call | tf_op jit(solution)/shard_map/pallas_call | solution.py:107
  2.3 16.5 %all-to-all-start = ((bf16[8,72,256]{2,1,0:T(8,128)(2,1)}), bf16[8,72,256]{2,1,0:T(8,128)(2,1)S(1)}, u32[]{:S(2)}, u32[]{:S(2)}) async-start(bf16[8,72,256]{2,1,0:T(8,128)(2,1)} %shard_map.100), calls=%async_computation | async-start | bytes 589824 | tf_op jit(solution)/shard_map/all_to_all | solution.py:18
  22.8 1.7 all-to-all-done
  25.7 5.4 %all-to-all-start.1 = ((bf16[8,64,128]{2,1,0:T(8,128)(2,1)}), bf16[8,64,128]{2,1,0:T(8,128)(2,1)S(1)}, u32[]{:S(2)}, u32[]{:S(2)}) async-start(bf16[8,64,128]{2,1,0:T(8,128)(2,1)} %broadcast_in_dim.68), calls=%async_computation.1 | async-start | bytes 262144 | tf_op jit(solution)/shard_map/all_to_all | solution.py:18
  31.1 4.0 %all-to-all-done.1 = bf16[8,64,128]{2,1,0:T(8,128)(2,1)S(1)} async-done(((bf16[8,64,128]{2,1,0:T(8,128)(2,1)}), bf16[8,64,128]{2,1,0:T(8,128)(2,1)S(1)}, u32[]{:S(2)}, u32[]{:S(2)}) %all-to-all-start.1) | async-done | bytes 131104 | tf_op jit(solution)/shard_map/all_to_all | solution.py:18
  36.2 7.2 %all-to-all-start.2 = ((bf16[16,64,256]{2,1,0:T(8,128)(2,1)}), bf16[16,64,256]{2,1,0:T(8,128)(2,1)S(1)}, u32[]{:S(2)}, u32[]{:S(2)}) async-start(bf16[16,64,256]{2,1,0:T(8,128)(2,1)} %bitcast.12), calls=%async_computation.2 | async-start | bytes 1048576 | tf_op jit(solution)/shard_map/all_to_all | solution.py:18
  44.4 6.2 %collective-permute-start = (bf16[1,288,512]{2,1,0:T(8,128)(2,1)S(1)}, bf16[1,288,512]{2,1,0:T(8,128)(2,1)S(1)}, u32[]{:S(2)}, u32[]{:S(2)}) collective-permute-start(bf16[1,288,512]{2,1,0:T(8,128)(2,1)S(1)} %bitcast.92), channel_id=1, source_target_pairs={{16,0},{24,8},{32,16},{40,24},{48,32},{56,40},{0,48},{8,56},{17,1}... | collective-permute-start | bytes 884744 | tf_op jit(solution)/shard_map/ppermute | solution.py:36
  50.6 1.9 collective-permute-start.1
  52.5 6.4 %collective-permute-start.2 = (bf16[1,288,512]{2,1,0:T(8,128)(2,1)S(1)}, bf16[1,288,512]{2,1,0:T(8,128)(2,1)S(1)}, u32[]{:S(2)}, u32[]{:S(2)}) collective-permute-start(bf16[1,288,512]{2,1,0:T(8,128)(2,1)S(1)} %bitcast.94), channel_id=1, source_target_pairs={{32,0},{40,8},{48,16},{56,24},{0,32},{8,40},{16,48},{24,56},{33,1}... | collective-permute-start | bytes 884744 | tf_op jit(solution)/shard_map/ppermute | solution.py:36
  61.4 14.0 %collective-permute-done = bf16[1,288,512]{2,1,0:T(8,128)(2,1)S(1)} collective-permute-done((bf16[1,288,512]{2,1,0:T(8,128)(2,1)S(1)}, bf16[1,288,512]{2,1,0:T(8,128)(2,1)S(1)}, u32[]{:S(2)}, u32[]{:S(2)}) %collective-permute-start) | collective-permute-done | bytes 294944 | tf_op jit(solution)/shard_map/ppermute | solution.py:36
  76.3 3.0 %collective-permute-start.3 = (bf16[2,288,512]{2,1,0:T(8,128)(2,1)}, bf16[2,288,512]{2,1,0:T(8,128)(2,1)S(1)}, u32[]{:S(2)}, u32[]{:S(2)}) collective-permute-start(bf16[2,288,512]{2,1,0:T(8,128)(2,1)} %get-tuple-element.14), channel_id=1, source_target_pairs={{8,0},{16,8},{24,16},{32,24},{40,32},{48,40},{56,48},{0,56},{9,1},... | collective-permute-start | bytes 1769480 | tf_op jit(solution)/shard_map/ppermute | solution.py:36
  79.3 2.9 %collective-permute-start.4 = (bf16[2,288,512]{2,1,0:T(8,128)(2,1)S(1)}, bf16[2,288,512]{2,1,0:T(8,128)(2,1)S(1)}, u32[]{:S(2)}, u32[]{:S(2)}) collective-permute-start(bf16[2,288,512]{2,1,0:T(8,128)(2,1)S(1)} %get-tuple-element.13), channel_id=1, source_target_pairs={{56,0},{0,8},{8,16},{16,24},{24,32},{32,40},{40,48},{48,56},{57,1}... | collective-permute-start | bytes 1769480 | tf_op jit(solution)/shard_map/ppermute | solution.py:36
  84.5 9.5 %all-to-all-start.3 = ((bf16[8,16,256]{2,1,0:T(8,128)(2,1)}), bf16[8,16,256]{2,1,0:T(8,128)(2,1)S(1)}, u32[]{:S(2)}, u32[]{:S(2)}) async-start(bf16[8,16,256]{2,1,0:T(8,128)(2,1)} %maximum_maximum_fusion.1), calls=%async_computation.3 | async-start | bytes 131072 | tf_op jit(solution)/shard_map/all_to_all | solution.py:18
  94.7 9.6 %all-to-all-done.3 = bf16[8,16,256]{2,1,0:T(8,128)(2,1)S(1)} async-done(((bf16[8,16,256]{2,1,0:T(8,128)(2,1)}), bf16[8,16,256]{2,1,0:T(8,128)(2,1)S(1)}, u32[]{:S(2)}, u32[]{:S(2)}) %all-to-all-start.3) | async-done | bytes 65568 | tf_op jit(solution)/shard_map/all_to_all | solution.py:18
  105.1 11.7 %all-to-all-start.4 = ((bf16[16,16,256]{2,1,0:T(8,128)(2,1)}), bf16[16,16,256]{2,1,0:T(8,128)(2,1)S(1)}, u32[]{:S(2)}, u32[]{:S(2)}) async-start(bf16[16,16,256]{2,1,0:T(8,128)(2,1)} %broadcast_in_dim.72), calls=%async_computation.4 | async-start | bytes 262144 | tf_op jit(solution)/shard_map/all_to_all | solution.py:18
  119.6 11.2 %all-to-all-done.4 = bf16[16,16,256]{2,1,0:T(8,128)(2,1)S(1)} async-done(((bf16[16,16,256]{2,1,0:T(8,128)(2,1)}), bf16[16,16,256]{2,1,0:T(8,128)(2,1)S(1)}, u32[]{:S(2)}, u32[]{:S(2)}) %all-to-all-start.4) | async-done | bytes 131104 | tf_op jit(solution)/shard_map/all_to_all | solution.py:18
  131.0 3.1 %fusion.11 = bf16[8,72,256]{2,1,0:T(8,128)(2,1)} fusion(bf16[8,288,512]{2,1,0:T(8,128)(2,1)} %constant_dynamic-update-slice_fusion.3, bf16[72]{0:T(256)(128)(2,1)S(1)} %get-tuple-element.50, bf16[72]{0:T(256)(128)(2,1)S(1)} %get-tuple-element.49, pred[256]{0:T(512)(128)(4,1)S(1)} %get-tuple-element.53, pred[256]{0:T(512)(128)(4,1)S(1)} %get-tuple-element.54, ...), kind=kOutput, calls=%fused_computation.6 | convolution fusion | flops 151400448 | bytes 2468640 | tf_op jit(solution)/shard_map/td,ykd->ytk/dot_general | solution.py:225
  134.0 5.4 %all-to-all-start.5 = ((bf16[8,72,256]{2,1,0:T(8,128)(2,1)}), bf16[8,72,256]{2,1,0:T(8,128)(2,1)S(1)}, u32[]{:S(2)}, u32[]{:S(2)}) async-start(bf16[8,72,256]{2,1,0:T(8,128)(2,1)} %fusion.11), calls=%async_computation.5 | async-start | bytes 589824 | tf_op jit(solution)/shard_map/all_to_all | solution.py:18
  139.5 5.8 %all-to-all-done.5 = bf16[8,72,256]{2,1,0:T(8,128)(2,1)S(1)} async-done(((bf16[8,72,256]{2,1,0:T(8,128)(2,1)}), bf16[8,72,256]{2,1,0:T(8,128)(2,1)S(1)}, u32[]{:S(2)}, u32[]{:S(2)}) %all-to-all-start.5) | async-done | bytes 294944 | tf_op jit(solution)/shard_map/all_to_all | solution.py:18
  145.8 8.5 %all_to_all.50 = bf16[8,64,128]{2,1,0:T(8,128)(2,1)S(1)} all-to-all(bf16[8,64,128]{2,1,0:T(8,128)(2,1)S(1)} %broadcast_in_dim.77), channel_id=1, replica_groups=mesh['ra_0'=16,'ra_1'=8,'cb'=8] {'cb'}, dimensions={0} | all-to-all | bytes 262144 | tf_op jit(solution)/shard_map/all_to_all | solution.py:18
  156.4 3.5 %all-to-all-start.7 = ((bf16[16,4,512]{2,1,0:T(4,128)(2,1)}), bf16[16,4,512]{2,1,0:T(4,128)(2,1)S(1)}, u32[]{:S(2)}, u32[]{:S(2)}) async-start(bf16[16,4,512]{2,1,0:T(4,128)(2,1)} %reshape.95), calls=%async_computation.7 | async-start | bytes 131072 | tf_op jit(solution)/shard_map/all_to_all | solution.py:18
  159.9 12.8 %all-to-all-done.7 = bf16[16,4,512]{2,1,0:T(4,128)(2,1)S(1)} async-done(((bf16[16,4,512]{2,1,0:T(4,128)(2,1)}), bf16[16,4,512]{2,1,0:T(4,128)(2,1)S(1)}, u32[]{:S(2)}, u32[]{:S(2)}) %all-to-all-start.7) | async-done | bytes 65568 | tf_op jit(solution)/shard_map/all_to_all | solution.py:18
  172.7 15.5 %all_to_all.51 = bf16[16,4,512]{2,1,0:T(4,128)(2,1)S(1)} all-to-all(bf16[16,4,512]{2,1,0:T(4,128)(2,1)S(1)} %broadcast_in_dim.78), channel_id=1, replica_groups=mesh['ra_0'=16,'ra_1'=8,'cb'=8] {'ra_0'}, dimensions={0} | all-to-all | bytes 131072 | tf_op jit(solution)/shard_map/all_to_all | solution.py:18
  188.3 18.4 %all_to_all.52 = bf16[8,64,512]{2,1,0:T(8,128)(2,1)S(1)} all-to-all(bf16[8,64,512]{2,1,0:T(8,128)(2,1)S(1)} %broadcast_in_dim.80), channel_id=1, replica_groups=mesh['ra_0'=16,'ra_1'=8,'cb'=8] {'ra_1'}, dimensions={0} | all-to-all | bytes 1048576 | tf_op jit(solution)/shard_map/all_to_all | solution.py:18
  (89 shorter events, 20.9 us)
Async XLA Ops:
  0.0 21.8 %copy-start = (f32[2,88,512]{2,1,0:T(8,128)S(1)}, f32[2,88,512]{2,1,0:T(8,128)}, u32[]{:S(2)}) copy-start(f32[2,88,512]{2,1,0:T(8,128)} %param.13) | copy-start | bytes 1081348
  2.3 22.2 %all-to-all-start = ((bf16[8,72,256]{2,1,0:T(8,128)(2,1)}), bf16[8,72,256]{2,1,0:T(8,128)(2,1)S(1)}, u32[]{:S(2)}, u32[]{:S(2)}) async-start(bf16[8,72,256]{2,1,0:T(8,128)(2,1)} %shard_map.100), calls=%async_computation | async-start | bytes 589824 | tf_op jit(solution)/shard_map/all_to_all | solution.py:18
  22.8 37.7 %copy-start.2 = (f32[2,512]{1,0:T(2,128)S(1)}, f32[2,512]{1,0:T(2,128)}, u32[]{:S(2)}) copy-start(f32[2,512]{1,0:T(2,128)} %param.16) | copy-start | bytes 12292
  22.8 37.9 %copy-start.1 = (f32[2,512]{1,0:T(2,128)S(1)}, f32[2,512]{1,0:T(2,128)}, u32[]{:S(2)}) copy-start(f32[2,512]{1,0:T(2,128)} %gain_ref.1) | copy-start | bytes 12292
  25.7 9.4 %all-to-all-start.1 = ((bf16[8,64,128]{2,1,0:T(8,128)(2,1)}), bf16[8,64,128]{2,1,0:T(8,128)(2,1)S(1)}, u32[]{:S(2)}, u32[]{:S(2)}) async-start(bf16[8,64,128]{2,1,0:T(8,128)(2,1)} %broadcast_in_dim.68), calls=%async_computation.1 | async-start | bytes 262144 | tf_op jit(solution)/shard_map/all_to_all | solution.py:18
  36.2 47.3 %all-to-all-start.2 = ((bf16[16,64,256]{2,1,0:T(8,128)(2,1)}), bf16[16,64,256]{2,1,0:T(8,128)(2,1)S(1)}, u32[]{:S(2)}, u32[]{:S(2)}) async-start(bf16[16,64,256]{2,1,0:T(8,128)(2,1)} %bitcast.12), calls=%async_computation.2 | async-start | bytes 1048576 | tf_op jit(solution)/shard_map/all_to_all | solution.py:18
  44.4 30.9 %collective-permute-start = (bf16[1,288,512]{2,1,0:T(8,128)(2,1)S(1)}, bf16[1,288,512]{2,1,0:T(8,128)(2,1)S(1)}, u32[]{:S(2)}, u32[]{:S(2)}) collective-permute-start(bf16[1,288,512]{2,1,0:T(8,128)(2,1)S(1)} %bitcast.92), channel_id=1, source_target_pairs={{16,0},{24,8},{32,16},{40,24},{48,32},{56,40},{0,48},{8,56},{17,1}... | collective-permute-start | bytes 884744 | tf_op jit(solution)/shard_map/ppermute | solution.py:36
  50.6 24.8 %collective-permute-start.1 = (bf16[1,288,512]{2,1,0:T(8,128)(2,1)S(1)}, bf16[1,288,512]{2,1,0:T(8,128)(2,1)S(1)}, u32[]{:S(2)}, u32[]{:S(2)}) collective-permute-start(bf16[1,288,512]{2,1,0:T(8,128)(2,1)S(1)} %bitcast.93), channel_id=1, source_target_pairs={{48,0},{56,8},{0,16},{8,24},{16,32},{24,40},{32,48},{40,56},{49,1}... | collective-permute-start | bytes 884744 | tf_op jit(solution)/shard_map/ppermute | solution.py:36
  52.5 41.4 %collective-permute-start.2 = (bf16[1,288,512]{2,1,0:T(8,128)(2,1)S(1)}, bf16[1,288,512]{2,1,0:T(8,128)(2,1)S(1)}, u32[]{:S(2)}, u32[]{:S(2)}) collective-permute-start(bf16[1,288,512]{2,1,0:T(8,128)(2,1)S(1)} %bitcast.94), channel_id=1, source_target_pairs={{32,0},{40,8},{48,16},{56,24},{0,32},{8,40},{16,48},{24,56},{33,1}... | collective-permute-start | bytes 884744 | tf_op jit(solution)/shard_map/ppermute | solution.py:36
  76.3 40.5 %collective-permute-start.3 = (bf16[2,288,512]{2,1,0:T(8,128)(2,1)}, bf16[2,288,512]{2,1,0:T(8,128)(2,1)S(1)}, u32[]{:S(2)}, u32[]{:S(2)}) collective-permute-start(bf16[2,288,512]{2,1,0:T(8,128)(2,1)} %get-tuple-element.14), channel_id=1, source_target_pairs={{8,0},{16,8},{24,16},{32,24},{40,32},{48,40},{56,48},{0,56},{9,1},... | collective-permute-start | bytes 1769480 | tf_op jit(solution)/shard_map/ppermute | solution.py:36
  79.3 38.4 %collective-permute-start.4 = (bf16[2,288,512]{2,1,0:T(8,128)(2,1)S(1)}, bf16[2,288,512]{2,1,0:T(8,128)(2,1)S(1)}, u32[]{:S(2)}, u32[]{:S(2)}) collective-permute-start(bf16[2,288,512]{2,1,0:T(8,128)(2,1)S(1)} %get-tuple-element.13), channel_id=1, source_target_pairs={{56,0},{0,8},{8,16},{16,24},{24,32},{32,40},{40,48},{48,56},{57,1}... | collective-permute-start | bytes 1769480 | tf_op jit(solution)/shard_map/ppermute | solution.py:36
  84.5 19.8 %all-to-all-start.3 = ((bf16[8,16,256]{2,1,0:T(8,128)(2,1)}), bf16[8,16,256]{2,1,0:T(8,128)(2,1)S(1)}, u32[]{:S(2)}, u32[]{:S(2)}) async-start(bf16[8,16,256]{2,1,0:T(8,128)(2,1)} %maximum_maximum_fusion.1), calls=%async_computation.3 | async-start | bytes 131072 | tf_op jit(solution)/shard_map/all_to_all | solution.py:18
  105.1 25.7 %all-to-all-start.4 = ((bf16[16,16,256]{2,1,0:T(8,128)(2,1)}), bf16[16,16,256]{2,1,0:T(8,128)(2,1)S(1)}, u32[]{:S(2)}, u32[]{:S(2)}) async-start(bf16[16,16,256]{2,1,0:T(8,128)(2,1)} %broadcast_in_dim.72), calls=%async_computation.4 | async-start | bytes 262144 | tf_op jit(solution)/shard_map/all_to_all | solution.py:18
  134.0 11.2 %all-to-all-start.5 = ((bf16[8,72,256]{2,1,0:T(8,128)(2,1)}), bf16[8,72,256]{2,1,0:T(8,128)(2,1)S(1)}, u32[]{:S(2)}, u32[]{:S(2)}) async-start(bf16[8,72,256]{2,1,0:T(8,128)(2,1)} %fusion.11), calls=%async_computation.5 | async-start | bytes 589824 | tf_op jit(solution)/shard_map/all_to_all | solution.py:18
  156.4 16.3 %all-to-all-start.7 = ((bf16[16,4,512]{2,1,0:T(4,128)(2,1)}), bf16[16,4,512]{2,1,0:T(4,128)(2,1)S(1)}, u32[]{:S(2)}, u32[]{:S(2)}) async-start(bf16[16,4,512]{2,1,0:T(4,128)(2,1)} %reshape.95), calls=%async_computation.7 | async-start | bytes 131072 | tf_op jit(solution)/shard_map/all_to_all | solution.py:18

commit v7 on v6

--- a/solution.py
+++ b/solution.py
@@ -61,7 +61,7 @@
 def split_in_three(value):
     first, rest = split_in_two(value)
     second, third = split_in_two(rest)
-    return tuple(part.astype(jnp.bfloat16) for part in (first, second, third))
+    return jnp.concatenate([first, second, third], axis=0).astype(jnp.bfloat16)
 
 
 def with_squares(product, squares, hidden):
@@ -157,20 +157,18 @@
     f32, bf16 = jnp.float32, jnp.bfloat16
 
     params_1 = own_params(conv_taps[1], conv_bias[1], gate_scale[1], up_scale[1])
-    carried = split_in_three(padded_to(padded_to(params_1, TILE, 0), width, 1))
+    carried = padded_to(split_in_three(padded_to(params_1, TILE, 0)), width, 1)
     packed = jnp.concatenate(
         [
             gate_weight[1].T.astype(bf16),
-            carried[0],
+            carried,
             up_weight[1].T.astype(bf16),
-            carried[1],
-            carried[2],
             down_weight[1].astype(bf16),
         ],
         axis=0,
     )
-    up_at = hidden + TILE
-    down_at = 2 * hidden + 3 * TILE
+    up_at = hidden + 3 * TILE
+    down_at = up_at + hidden
     packed = gathered_in_steps(packed[None], "ra_1")
 
     params_0 = own_params(conv_taps[0], conv_bias[0], gate_scale[0], up_scale[0])
@@ -228,12 +226,8 @@
     product = with_squares(product, squares[None], hidden).astype(bf16)
     total = swapped(product, "cb").astype(f32).sum(axis=0)
     theirs = lax.dynamic_index_in_dim(packed, lax.axis_index("cb"), 0, keepdims=False)
-    theirs = theirs[:, :LANES].astype(f32)
-    theirs = (
-        theirs[hidden:up_at]
-        + theirs[down_at - 2 * TILE : down_at - TILE]
-        + theirs[down_at - TILE : down_at]
-    )
+    theirs = theirs[hidden:up_at, :LANES].astype(f32).reshape(3, TILE, LANES)
+    theirs = theirs[0] + theirs[1] + theirs[2]
     inner = activated(total, features, hidden, up_at, theirs)
     inner = sent_to_all(inner, "cb")
     down_1 = packed[:, down_at:]

time: 210 us -> 210 us (level)
    unnamed x18 -> x15, local copies, waits for them, and re-layouts: 6.48 us -> 3.89 us
where the time goes in v7:
time: 210 us; the launch traced here: 208 us
  starting transfers between devices  79.5 us (38%)
  waiting for transfers between devices  59.9 us (29%)
  blocking collectives  42.5 us (20%)
  local copies, waits for them, and re-layouts  13.2 us (6%)
  other arithmetic  5.16 us (2%)
  matrix products  4.73 us (2%)
  Pallas kernels  2.25 us (1%)
    all_to_all x7, starting transfers between devices, swapped(): return lax.all_to_all(pieces, axes, 0, 0, tiled=True)  59.2 us
    all_to_all x7, waiting for transfers between devices, swapped(): return lax.all_to_all(pieces, axes, 0, 0, tiled=True)  46 us
    all_to_all x3, blocking collectives, swapped(): return lax.all_to_all(pieces, axes, 0, 0, tiled=True)  42.5 us
    ppermute x5, starting transfers between devices, taken_from(): lax.ppermute(value, axis, [((i + away) % size, i) for i in range(size)])  20.3 us
    ppermute x5, waiting for transfers between devices, taken_from(): lax.ppermute(value, axis, [((i + away) % size, i) for i in range(size)])  14 us
  transfers between devices with their start and end apart: 12, of which 7 were waited for; matrix products, arithmetic and copies ran while one was open for 7% of the time, Pallas kernels for 0%

profile of v7, /device:TPU:6, one launch (start us, length us, event | category | flops | bytes accessed | tf_op | source)
XLA Modules:
  0.0 207.7 jit_solution(8178163651981317244)
XLA Ops:
  0.0 2.2 %shard_map.100 = bf16[8,72,256]{2,1,0:T(8,128)(2,1)} custom-call(bf16[512,512]{1,0:T(8,128)(2,1)} %tokens_ref.1, f32[2,512]{1,0:T(2,128)} %gain_ref.1, f32[2,88,512]{2,1,0:T(8,128)} %bitcast.88, f32[2,88,512]{2,1,0:T(8,128)} %bitcast.89), custom_call_target="tpu_custom_call" | custom-call | tf_op jit(solution)/shard_map/pallas_call | solution.py:107
  2.3 16.5 %all-to-all-start = ((bf16[8,72,256]{2,1,0:T(8,128)(2,1)}), bf16[8,72,256]{2,1,0:T(8,128)(2,1)S(1)}, u32[]{:S(2)}, u32[]{:S(2)}) async-start(bf16[8,72,256]{2,1,0:T(8,128)(2,1)} %shard_map.100), calls=%async_computation | async-start | bytes 589824 | tf_op jit(solution)/shard_map/all_to_all | solution.py:18
  21.8 2.7 %all-to-all-done = bf16[8,72,256]{2,1,0:T(8,128)(2,1)S(1)} async-done(((bf16[8,72,256]{2,1,0:T(8,128)(2,1)}), bf16[8,72,256]{2,1,0:T(8,128)(2,1)S(1)}, u32[]{:S(2)}, u32[]{:S(2)}) %all-to-all-start) | async-done | bytes 294944 | tf_op jit(solution)/shard_map/all_to_all | solution.py:18
  25.7 5.4 %all-to-all-start.1 = ((bf16[8,64,128]{2,1,0:T(8,128)(2,1)}), bf16[8,64,128]{2,1,0:T(8,128)(2,1)S(1)}, u32[]{:S(2)}, u32[]{:S(2)}) async-start(bf16[8,64,128]{2,1,0:T(8,128)(2,1)} %broadcast_in_dim.68), calls=%async_computation.1 | async-start | bytes 262144 | tf_op jit(solution)/shard_map/all_to_all | solution.py:18
  31.1 4.0 %all-to-all-done.1 = bf16[8,64,128]{2,1,0:T(8,128)(2,1)S(1)} async-done(((bf16[8,64,128]{2,1,0:T(8,128)(2,1)}), bf16[8,64,128]{2,1,0:T(8,128)(2,1)S(1)}, u32[]{:S(2)}, u32[]{:S(2)}) %all-to-all-start.1) | async-done | bytes 131104 | tf_op jit(solution)/shard_map/all_to_all | solution.py:18
  36.3 7.2 %all-to-all-start.2 = ((bf16[16,64,256]{2,1,0:T(8,128)(2,1)}), bf16[16,64,256]{2,1,0:T(8,128)(2,1)S(1)}, u32[]{:S(2)}, u32[]{:S(2)}) async-start(bf16[16,64,256]{2,1,0:T(8,128)(2,1)} %bitcast.12), calls=%async_computation.2 | async-start | bytes 1048576 | tf_op jit(solution)/shard_map/all_to_all | solution.py:18
  44.6 6.2 %collective-permute-start = (bf16[1,288,512]{2,1,0:T(8,128)(2,1)S(1)}, bf16[1,288,512]{2,1,0:T(8,128)(2,1)S(1)}, u32[]{:S(2)}, u32[]{:S(2)}) collective-permute-start(bf16[1,288,512]{2,1,0:T(8,128)(2,1)S(1)} %maximum_bitcast_fusion), channel_id=1, source_target_pairs={{16,0},{24,8},{32,16},{40,24},{48,32},{56,40},{0,48},{8,56},{17,1}... | collective-permute-start | bytes 884744 | tf_op jit(solution)/shard_map/ppermute | solution.py:36
  50.7 1.9 collective-permute-start.1
  52.6 6.4 %collective-permute-start.2 = (bf16[1,288,512]{2,1,0:T(8,128)(2,1)S(1)}, bf16[1,288,512]{2,1,0:T(8,128)(2,1)S(1)}, u32[]{:S(2)}, u32[]{:S(2)}) collective-permute-start(bf16[1,288,512]{2,1,0:T(8,128)(2,1)S(1)} %maximum_bitcast_fusion), channel_id=1, source_target_pairs={{32,0},{40,8},{48,16},{56,24},{0,32},{8,40},{16,48},{24,56},{33,1}... | collective-permute-start | bytes 884744 | tf_op jit(solution)/shard_map/ppermute | solution.py:36
  61.5 13.9 %collective-permute-done = bf16[1,288,512]{2,1,0:T(8,128)(2,1)S(1)} collective-permute-done((bf16[1,288,512]{2,1,0:T(8,128)(2,1)S(1)}, bf16[1,288,512]{2,1,0:T(8,128)(2,1)S(1)}, u32[]{:S(2)}, u32[]{:S(2)}) %collective-permute-start) | collective-permute-done | bytes 294944 | tf_op jit(solution)/shard_map/ppermute | solution.py:36
  76.4 3.0 %collective-permute-start.3 = (bf16[2,288,512]{2,1,0:T(8,128)(2,1)}, bf16[2,288,512]{2,1,0:T(8,128)(2,1)S(1)}, u32[]{:S(2)}, u32[]{:S(2)}) collective-permute-start(bf16[2,288,512]{2,1,0:T(8,128)(2,1)} %get-tuple-element.14), channel_id=1, source_target_pairs={{8,0},{16,8},{24,16},{32,24},{40,32},{48,40},{56,48},{0,56},{9,1},... | collective-permute-start | bytes 1769480 | tf_op jit(solution)/shard_map/ppermute | solution.py:36
  79.4 2.8 %collective-permute-start.4 = (bf16[2,288,512]{2,1,0:T(8,128)(2,1)S(1)}, bf16[2,288,512]{2,1,0:T(8,128)(2,1)S(1)}, u32[]{:S(2)}, u32[]{:S(2)}) collective-permute-start(bf16[2,288,512]{2,1,0:T(8,128)(2,1)S(1)} %get-tuple-element.13), channel_id=1, source_target_pairs={{56,0},{0,8},{8,16},{16,24},{24,32},{32,40},{40,48},{48,56},{57,1}... | collective-permute-start | bytes 1769480 | tf_op jit(solution)/shard_map/ppermute | solution.py:36
  84.6 9.5 %all-to-all-start.3 = ((bf16[8,16,256]{2,1,0:T(8,128)(2,1)}), bf16[8,16,256]{2,1,0:T(8,128)(2,1)S(1)}, u32[]{:S(2)}, u32[]{:S(2)}) async-start(bf16[8,16,256]{2,1,0:T(8,128)(2,1)} %maximum_maximum_fusion.1), calls=%async_computation.3 | async-start | bytes 131072 | tf_op jit(solution)/shard_map/all_to_all | solution.py:18
  94.8 9.6 %all-to-all-done.3 = bf16[8,16,256]{2,1,0:T(8,128)(2,1)S(1)} async-done(((bf16[8,16,256]{2,1,0:T(8,128)(2,1)}), bf16[8,16,256]{2,1,0:T(8,128)(2,1)S(1)}, u32[]{:S(2)}, u32[]{:S(2)}) %all-to-all-start.3) | async-done | bytes 65568 | tf_op jit(solution)/shard_map/all_to_all | solution.py:18
  105.2 11.7 %all-to-all-start.4 = ((bf16[16,16,256]{2,1,0:T(8,128)(2,1)}), bf16[16,16,256]{2,1,0:T(8,128)(2,1)S(1)}, u32[]{:S(2)}, u32[]{:S(2)}) async-start(bf16[16,16,256]{2,1,0:T(8,128)(2,1)} %broadcast_in_dim.72), calls=%async_computation.4 | async-start | bytes 262144 | tf_op jit(solution)/shard_map/all_to_all | solution.py:18
  119.7 11.2 %all-to-all-done.4 = bf16[16,16,256]{2,1,0:T(8,128)(2,1)S(1)} async-done(((bf16[16,16,256]{2,1,0:T(8,128)(2,1)}), bf16[16,16,256]{2,1,0:T(8,128)(2,1)S(1)}, u32[]{:S(2)}, u32[]{:S(2)}) %all-to-all-start.4) | async-done | bytes 131104 | tf_op jit(solution)/shard_map/all_to_all | solution.py:18
  131.1 3.1 %fusion.11 = bf16[8,72,256]{2,1,0:T(8,128)(2,1)} fusion(bf16[8,288,512]{2,1,0:T(8,128)(2,1)} %constant_dynamic-update-slice_fusion, bf16[72]{0:T(256)(128)(2,1)S(1)} %get-tuple-element.55, bf16[72]{0:T(256)(128)(2,1)S(1)} %get-tuple-element.54, pred[256]{0:T(512)(128)(4,1)S(1)} %get-tuple-element.60, pred[256]{0:T(512)(128)(4,1)S(1)} %get-tuple-element.61, ...), kind=kOutput, calls=%fused_computation.6 | convolution fusion | flops 151400448 | bytes 2468640 | tf_op jit(solution)/shard_map/td,ykd->ytk/dot_general | solution.py:223
  134.2 5.4 %all-to-all-start.5 = ((bf16[8,72,256]{2,1,0:T(8,128)(2,1)}), bf16[8,72,256]{2,1,0:T(8,128)(2,1)S(1)}, u32[]{:S(2)}, u32[]{:S(2)}) async-start(bf16[8,72,256]{2,1,0:T(8,128)(2,1)} %fusion.11), calls=%async_computation.5 | async-start | bytes 589824 | tf_op jit(solution)/shard_map/all_to_all | solution.py:18
  139.6 5.8 %all-to-all-done.5 = bf16[8,72,256]{2,1,0:T(8,128)(2,1)S(1)} async-done(((bf16[8,72,256]{2,1,0:T(8,128)(2,1)}), bf16[8,72,256]{2,1,0:T(8,128)(2,1)S(1)}, u32[]{:S(2)}, u32[]{:S(2)}) %all-to-all-start.5) | async-done | bytes 294944 | tf_op jit(solution)/shard_map/all_to_all | solution.py:18
  146.0 8.5 %all_to_all.50 = bf16[8,64,128]{2,1,0:T(8,128)(2,1)S(1)} all-to-all(bf16[8,64,128]{2,1,0:T(8,128)(2,1)S(1)} %broadcast_in_dim.77), channel_id=1, replica_groups=mesh['ra_0'=16,'ra_1'=8,'cb'=8] {'cb'}, dimensions={0} | all-to-all | bytes 262144 | tf_op jit(solution)/shard_map/all_to_all | solution.py:18
  156.5 3.5 %all-to-all-start.7 = ((bf16[16,4,512]{2,1,0:T(4,128)(2,1)}), bf16[16,4,512]{2,1,0:T(4,128)(2,1)S(1)}, u32[]{:S(2)}, u32[]{:S(2)}) async-start(bf16[16,4,512]{2,1,0:T(4,128)(2,1)} %reshape.102), calls=%async_computation.7 | async-start | bytes 131072 | tf_op jit(solution)/shard_map/all_to_all | solution.py:18
  160.0 12.8 %all-to-all-done.7 = bf16[16,4,512]{2,1,0:T(4,128)(2,1)S(1)} async-done(((bf16[16,4,512]{2,1,0:T(4,128)(2,1)}), bf16[16,4,512]{2,1,0:T(4,128)(2,1)S(1)}, u32[]{:S(2)}, u32[]{:S(2)}) %all-to-all-start.7) | async-done | bytes 65568 | tf_op jit(solution)/shard_map/all_to_all | solution.py:18
  172.9 15.5 %all_to_all.51 = bf16[16,4,512]{2,1,0:T(4,128)(2,1)S(1)} all-to-all(bf16[16,4,512]{2,1,0:T(4,128)(2,1)S(1)} %broadcast_in_dim.78), channel_id=1, replica_groups=mesh['ra_0'=16,'ra_1'=8,'cb'=8] {'ra_0'}, dimensions={0} | all-to-all | bytes 131072 | tf_op jit(solution)/shard_map/all_to_all | solution.py:18
  188.5 18.4 %all_to_all.52 = bf16[8,64,512]{2,1,0:T(8,128)(2,1)S(1)} all-to-all(bf16[8,64,512]{2,1,0:T(8,128)(2,1)S(1)} %broadcast_in_dim.80), channel_id=1, replica_groups=mesh['ra_0'=16,'ra_1'=8,'cb'=8] {'ra_1'}, dimensions={0} | all-to-all | bytes 1048576 | tf_op jit(solution)/shard_map/all_to_all | solution.py:18
  (87 shorter events, 20.1 us)
Async XLA Ops:
  0.0 21.8 %copy-start = (f32[2,88,512]{2,1,0:T(8,128)S(1)}, f32[2,88,512]{2,1,0:T(8,128)}, u32[]{:S(2)}) copy-start(f32[2,88,512]{2,1,0:T(8,128)} %param.13) | copy-start | bytes 1081348
  2.3 22.2 %all-to-all-start = ((bf16[8,72,256]{2,1,0:T(8,128)(2,1)}), bf16[8,72,256]{2,1,0:T(8,128)(2,1)S(1)}, u32[]{:S(2)}, u32[]{:S(2)}) async-start(bf16[8,72,256]{2,1,0:T(8,128)(2,1)} %shard_map.100), calls=%async_computation | async-start | bytes 589824 | tf_op jit(solution)/shard_map/all_to_all | solution.py:18
  25.0 34.2 %copy-start.1 = (f32[2,512]{1,0:T(2,128)S(1)}, f32[2,512]{1,0:T(2,128)}, u32[]{:S(2)}) copy-start(f32[2,512]{1,0:T(2,128)} %gain_ref.1) | copy-start | bytes 12292
  25.0 35.0 %copy-start.2 = (f32[2,512]{1,0:T(2,128)S(1)}, f32[2,512]{1,0:T(2,128)}, u32[]{:S(2)}) copy-start(f32[2,512]{1,0:T(2,128)} %param.16) | copy-start | bytes 12292
  25.7 9.4 %all-to-all-start.1 = ((bf16[8,64,128]{2,1,0:T(8,128)(2,1)}), bf16[8,64,128]{2,1,0:T(8,128)(2,1)S(1)}, u32[]{:S(2)}, u32[]{:S(2)}) async-start(bf16[8,64,128]{2,1,0:T(8,128)(2,1)} %broadcast_in_dim.68), calls=%async_computation.1 | async-start | bytes 262144 | tf_op jit(solution)/shard_map/all_to_all | solution.py:18
  36.3 47.5 %all-to-all-start.2 = ((bf16[16,64,256]{2,1,0:T(8,128)(2,1)}), bf16[16,64,256]{2,1,0:T(8,128)(2,1)S(1)}, u32[]{:S(2)}, u32[]{:S(2)}) async-start(bf16[16,64,256]{2,1,0:T(8,128)(2,1)} %bitcast.12), calls=%async_computation.2 | async-start | bytes 1048576 | tf_op jit(solution)/shard_map/all_to_all | solution.py:18
  44.6 30.9 %collective-permute-start = (bf16[1,288,512]{2,1,0:T(8,128)(2,1)S(1)}, bf16[1,288,512]{2,1,0:T(8,128)(2,1)S(1)}, u32[]{:S(2)}, u32[]{:S(2)}) collective-permute-start(bf16[1,288,512]{2,1,0:T(8,128)(2,1)S(1)} %maximum_bitcast_fusion), channel_id=1, source_target_pairs={{16,0},{24,8},{32,16},{40,24},{48,32},{56,40},{0,48},{8,56},{17,1}... | collective-permute-start | bytes 884744 | tf_op jit(solution)/shard_map/ppermute | solution.py:36
  50.7 24.8 %collective-permute-start.1 = (bf16[1,288,512]{2,1,0:T(8,128)(2,1)S(1)}, bf16[1,288,512]{2,1,0:T(8,128)(2,1)S(1)}, u32[]{:S(2)}, u32[]{:S(2)}) collective-permute-start(bf16[1,288,512]{2,1,0:T(8,128)(2,1)S(1)} %maximum_bitcast_fusion), channel_id=1, source_target_pairs={{48,0},{56,8},{0,16},{8,24},{16,32},{24,40},{32,48},{40,56},{49,1}... | collective-permute-start | bytes 884744 | tf_op jit(solution)/shard_map/ppermute | solution.py:36
  52.6 41.4 %collective-permute-start.2 = (bf16[1,288,512]{2,1,0:T(8,128)(2,1)S(1)}, bf16[1,288,512]{2,1,0:T(8,128)(2,1)S(1)}, u32[]{:S(2)}, u32[]{:S(2)}) collective-permute-start(bf16[1,288,512]{2,1,0:T(8,128)(2,1)S(1)} %maximum_bitcast_fusion), channel_id=1, source_target_pairs={{32,0},{40,8},{48,16},{56,24},{0,32},{8,40},{16,48},{24,56},{33,1}... | collective-permute-start | bytes 884744 | tf_op jit(solution)/shard_map/ppermute | solution.py:36
  76.4 40.5 %collective-permute-start.3 = (bf16[2,288,512]{2,1,0:T(8,128)(2,1)}, bf16[2,288,512]{2,1,0:T(8,128)(2,1)S(1)}, u32[]{:S(2)}, u32[]{:S(2)}) collective-permute-start(bf16[2,288,512]{2,1,0:T(8,128)(2,1)} %get-tuple-element.14), channel_id=1, source_target_pairs={{8,0},{16,8},{24,16},{32,24},{40,32},{48,40},{56,48},{0,56},{9,1},... | collective-permute-start | bytes 1769480 | tf_op jit(solution)/shard_map/ppermute | solution.py:36
  79.4 38.4 %collective-permute-start.4 = (bf16[2,288,512]{2,1,0:T(8,128)(2,1)S(1)}, bf16[2,288,512]{2,1,0:T(8,128)(2,1)S(1)}, u32[]{:S(2)}, u32[]{:S(2)}) collective-permute-start(bf16[2,288,512]{2,1,0:T(8,128)(2,1)S(1)} %get-tuple-element.13), channel_id=1, source_target_pairs={{56,0},{0,8},{8,16},{16,24},{24,32},{32,40},{40,48},{48,56},{57,1}... | collective-permute-start | bytes 1769480 | tf_op jit(solution)/shard_map/ppermute | solution.py:36
  84.6 19.8 %all-to-all-start.3 = ((bf16[8,16,256]{2,1,0:T(8,128)(2,1)}), bf16[8,16,256]{2,1,0:T(8,128)(2,1)S(1)}, u32[]{:S(2)}, u32[]{:S(2)}) async-start(bf16[8,16,256]{2,1,0:T(8,128)(2,1)} %maximum_maximum_fusion.1), calls=%async_computation.3 | async-start | bytes 131072 | tf_op jit(solution)/shard_map/all_to_all | solution.py:18
  105.2 25.7 %all-to-all-start.4 = ((bf16[16,16,256]{2,1,0:T(8,128)(2,1)}), bf16[16,16,256]{2,1,0:T(8,128)(2,1)S(1)}, u32[]{:S(2)}, u32[]{:S(2)}) async-start(bf16[16,16,256]{2,1,0:T(8,128)(2,1)} %broadcast_in_dim.72), calls=%async_computation.4 | async-start | bytes 262144 | tf_op jit(solution)/shard_map/all_to_all | solution.py:18
  134.2 11.2 %all-to-all-start.5 = ((bf16[8,72,256]{2,1,0:T(8,128)(2,1)}), bf16[8,72,256]{2,1,0:T(8,128)(2,1)S(1)}, u32[]{:S(2)}, u32[]{:S(2)}) async-start(bf16[8,72,256]{2,1,0:T(8,128)(2,1)} %fusion.11), calls=%async_computation.5 | async-start | bytes 589824 | tf_op jit(solution)/shard_map/all_to_all | solution.py:18
  156.5 16.3 %all-to-all-start.7 = ((bf16[16,4,512]{2,1,0:T(4,128)(2,1)}), bf16[16,4,512]{2,1,0:T(4,128)(2,1)S(1)}, u32[]{:S(2)}, u32[]{:S(2)}) async-start(bf16[16,4,512]{2,1,0:T(4,128)(2,1)} %reshape.102), calls=%async_computation.7 | async-start | bytes 131072 | tf_op jit(solution)/shard_map/all_to_all | solution.py:18
